TPU v7x, 128 devices: a whole 4x4x4 slice. The times are simulated.
128 devices in a mesh: ep: 32 (over z, y, core), tp: 4 (over x).
Axes of the slice: x: 4, y: 4, z: 4, core: 2. Of those that a mesh axis runs over, the one named last changes fastest.
Arguments:
- queries: bfloat16 [16384, 1024], P('ep', 'tp'), may hold values from -8 to 8
- key_rows: bfloat16 [16384, 1024], P('ep', 'tp'), may hold values from -8 to 8
- value_rows: bfloat16 [16384, 1024], P('ep', 'tp'), may hold values from -6 to 6
- lambdas: float32 [8], P('tp'), may hold values from 0.3 to 0.8
- head_gain: float32 [128], replicated, may hold values from 0.1 to 1.9
- out_weight: bfloat16 [1024, 2048], P('tp'), may hold values from -0.1875 to 0.1875
- moe_input: bfloat16 [16384, 2048], P(('ep', 'tp')), may hold values from -400 to 400
- moe_gain: float32 [2048], replicated, may hold values from 0.1 to 1.9
- routes: int32 [16384, 2], P(('ep', 'tp')), may hold values from 0 to 31, all different within a row; in each aligned block of 128 rows (0 to 127, 128 to 255, ...) at most 10 rows name the same one
- route_logits: float32 [16384, 2], P(('ep', 'tp')), may hold values from -6 to 6
- expert_gate: bfloat16 [32, 2048, 3584], P('ep', None, 'tp'), may hold values from -0.125 to 0.125
- expert_up: bfloat16 [32, 2048, 3584], P('ep', None, 'tp'), may hold values from -0.125 to 0.125
- expert_down: bfloat16 [32, 3584, 2048], P('ep', 'tp'), may hold values from -0.09375 to 0.09375
Outputs:
- mixer_out: bfloat16 [16384, 2048], P(('ep', 'tp'))
- expert_out: bfloat16 [16384, 2048], P(('ep', 'tp'))
Inputs may be any that keep to these rules, and one draw needn't show every extreme that they name: `routes`: each token names 2 different experts. Among the tokens of one device no expert is named more than 10 times, and in every draw some expert is named exactly 10 times by the tokens of some device.
All inputs are finite; a program needn't handle non-finite values.
Results may differ from a plain program's by a relative error of at most 0.014.
Values may be sent and summed in bfloat16 or wider, within the bound.
A program may use at most 128 MiB of HBM per device.

v0:
```python
import jax
import jax.numpy as jnp
from jax import lax
from jax.sharding import PartitionSpec as P

epsilon = 1e-06
init_lambda = 0.2


def side_by_side(arrays, axis, dim, along):
    widths = [a.shape[along] for a in arrays]
    both = jnp.concatenate(arrays, axis=along)
    result = lax.all_gather(both, axis, axis=dim, tiled=True)
    return tuple(jnp.split(result, [sum(widths[:k]) for k in range(1, len(widths))], axis=along))


def split_up(array, dim, devices):
    before, after = (array.shape[:dim], array.shape[dim + 1 :])
    return jnp.moveaxis(array.reshape(*before, devices, -1, *after), dim, 0)


def summed_on_arrival(array, axis, dim):
    devices = lax.axis_size(axis)
    blocks = lax.all_to_all(split_up(array, dim, devices), axis, 0, 0, tiled=True)
    return jnp.sum(blocks.astype(jnp.float32), axis=0)


def capacity(tokens, top_count, experts):
    return max(2, (top_count * tokens * 5 + 4 * experts - 1) // (4 * experts))


def per_device(
    queries,
    key_rows,
    value_rows,
    lambdas,
    head_gain,
    out_weight,
    moe_input,
    moe_gain,
    routes,
    route_logits,
    expert_gate,
    expert_up,
    expert_down,
):
    local_rows = queries.shape[0]
    local_heads = lambdas.shape[0]
    head_size = queries.shape[1] // (2 * local_heads)
    value_size = value_rows.shape[1] // local_heads
    model_width = out_weight.shape[1]
    score_scale = head_size ** (-0.5)
    query_maps = queries.reshape(local_rows, local_heads, 2, head_size)

    def attend_block(running, key_block, value_block):
        maxima, totals, accumulated = running
        key_count = key_block.shape[0]
        key_maps = key_block.reshape(key_count, local_heads, 2, head_size)
        value_heads = value_block.reshape(key_count, local_heads, value_size)
        scores = (
            jnp.einsum("qhid,khid->ihqk", query_maps, key_maps, preferred_element_type=jnp.float32)
            * score_scale
        )
        new_max = jnp.maximum(maxima, jnp.max(scores, axis=-1))
        weights = jnp.exp(scores - new_max[..., None])
        factor = jnp.exp(maxima - new_max)
        totals = totals * factor + jnp.sum(weights, axis=-1)
        accumulated = accumulated * factor[..., None] + jnp.einsum(
            "ihqk,khe->ihqe",
            weights.astype(jnp.bfloat16),
            value_heads,
            preferred_element_type=jnp.float32,
        )
        return (new_max, totals, accumulated)

    initial = (
        jnp.full((2, local_heads, local_rows), -1e30, jnp.float32),
        jnp.zeros((2, local_heads, local_rows), jnp.float32),
        jnp.zeros((2, local_heads, local_rows, value_size), jnp.float32),
    )
    key_piece, value_piece = side_by_side((key_rows, value_rows), "ep", 0, 1)
    length = key_piece.shape[0]
    block_rows = length
    while block_rows > 1024 and block_rows % 2 == 0:
        block_rows //= 2

    def loop_body(step_index, partial_state):
        first_row = step_index * block_rows
        return attend_block(
            partial_state,
            lax.dynamic_slice_in_dim(key_piece, first_row, block_rows, 0),
            lax.dynamic_slice_in_dim(value_piece, first_row, block_rows, 0),
        )

    maxima, totals, accumulated = lax.fori_loop(0, length // block_rows, loop_body, initial)
    maps_out = accumulated / totals[..., None]
    head_out = maps_out[0] - lambdas[:, None, None] * maps_out[1]
    mean_square = jnp.mean(head_out * head_out, axis=-1, keepdims=True)
    attended = (
        head_out * lax.rsqrt(mean_square + epsilon) * head_gain * (1.0 - init_lambda)
    ).astype(jnp.bfloat16)
    out_heads = out_weight.reshape(local_heads, value_size, model_width)
    token_count, top_count = routes.shape
    experts_all = lax.axis_size("ep")
    slot_count = capacity(token_count, top_count, experts_all)
    moe_float = moe_input.astype(jnp.float32)
    normed = (
        moe_float
        * lax.rsqrt(jnp.mean(moe_float * moe_float, axis=-1, keepdims=True) + epsilon)
        * moe_gain
    ).astype(jnp.bfloat16)
    gate_weights = jax.nn.softmax(route_logits, axis=-1)
    flat_routes = routes.reshape(-1)
    chosen = (flat_routes[:, None] == jnp.arange(experts_all, dtype=jnp.int32)[None, :]).astype(
        jnp.int32
    )
    slot_rank = jnp.sum((jnp.cumsum(chosen, axis=0) - chosen) * chosen, axis=1)
    slot_ids = (flat_routes * slot_count + slot_rank).reshape(token_count, top_count)
    dispatch = jnp.any(
        slot_ids[None, :, :]
        == jnp.arange(experts_all * slot_count, dtype=jnp.int32)[:, None, None],
        axis=-1,
    ).astype(jnp.bfloat16)
    outgoing = (
        jnp.dot(dispatch, normed, preferred_element_type=jnp.float32)
        .astype(jnp.bfloat16)
        .reshape(experts_all, slot_count, model_width)
    )
    gate_local = expert_gate[0]
    up_local = expert_up[0]
    down_local = expert_down[0]
    arrived = lax.all_to_all(outgoing, "ep", split_axis=0, concat_axis=0, tiled=True)
    segment = lax.all_gather(
        arrived.reshape(experts_all * slot_count, model_width), "tp", axis=0, tiled=True
    )
    gate_part = jnp.dot(segment, gate_local, preferred_element_type=jnp.float32)
    up_part = jnp.dot(segment, up_local, preferred_element_type=jnp.float32)
    hidden = (jax.nn.silu(gate_part) * up_part).astype(jnp.bfloat16)
    expert_slots = experts_all * slot_count
    mixer_sum = summed_on_arrival(
        jnp.einsum("hqe,hed->qd", attended, out_heads, preferred_element_type=jnp.float32).astype(
            jnp.bfloat16
        ),
        "tp",
        0,
    )
    expert_sum = summed_on_arrival(
        jnp.dot(hidden, down_local, preferred_element_type=jnp.float32).astype(jnp.bfloat16),
        "tp",
        0,
    )
    replies = lax.all_to_all(
        expert_sum.astype(jnp.bfloat16).reshape(experts_all, slot_count, model_width),
        "ep",
        split_axis=0,
        concat_axis=0,
        tiled=True,
    )
    picked = jnp.take(
        replies.reshape(expert_slots, model_width), slot_ids.reshape(-1), axis=0
    ).reshape(token_count, top_count, model_width)
    expert_out = jnp.sum(gate_weights[:, :, None] * picked.astype(jnp.float32), axis=1).astype(
        jnp.bfloat16
    )
    return (mixer_sum.astype(jnp.bfloat16), expert_out)


def solution(mesh):
    placed = (
        P("ep", "tp"),
        P("ep", "tp"),
        P("ep", "tp"),
        P("tp"),
        P(),
        P("tp", None),
        P(("ep", "tp"), None),
        P(),
        P(("ep", "tp"), None),
        P(("ep", "tp"), None),
        P("ep", None, "tp"),
        P("ep", None, "tp"),
        P("ep", "tp", None),
    )
    return jax.shard_map(
        per_device,
        mesh=mesh,
        in_specs=placed,
        out_specs=(P(("ep", "tp"), None), P(("ep", "tp"), None)),
        check_vma=False,
    )
```

profile of v0, /device:TPU:1, one launch (start us, length us, event | category | flops | bytes accessed | tf_op | source)
XLA Modules:
  0.0 373.2 jit_solution(11716625860648907072)
XLA Ops:
  11.5 2.7 convolution_convert_fusion.1
  14.2 2.3 reshape.140
  16.5 37.9 %all_to_all.20 = bf16[32,10,2048]{2,1,0:T(8,128)(2,1)} all-to-all(bf16[32,10,2048]{2,1,0:T(8,128)(2,1)S(1)} %reshape.140), channel_id=1, replica_groups=mesh['ep'=32,'tp'=4] {'ep'}, dimensions={0} | all-to-all | bytes 2621440 | tf_op jit(solution)/shard_map/all_to_all | solution.py:132
  54.4 3.6 reshape.141
  59.3 53.1 %all-gather.5.cloned.1.call-done = bf16[1280,2048]{1,0:T(8,128)(2,1)} async-done(((bf16[320,2048]{1,0:T(8,128)(2,1)}), bf16[1280,2048]{1,0:T(8,128)(2,1)}) %all-gather.5.cloned.1.call-update) | async-done | bytes 5242896 | tf_op jit(solution)/shard_map/all_gather | solution.py:133
  112.4 10.0 %fusion.17 = f32[1280,896]{1,0:T(8,128)} fusion(bf16[1280,2048]{1,0:T(8,128)(2,1)} %all-gather.5.cloned.1.call-done, bf16[1,2048,896]{2,1,0:T(8,128)(2,1)} %param.25), kind=kOutput, calls=%fused_computation.25 | convolution fusion | flops 4697620480 | bytes 13500416 | tf_op jit(solution)/shard_map/dot_general | solution.py:136
  122.4 17.9 %convolution_convert_fusion = bf16[1280,2048]{1,0:T(8,128)(2,1)} fusion(bf16[1,896,2048]{2,1,0:T(8,128)(2,1)} %param.27, f32[1280,896]{1,0:T(8,128)} %fusion.17, bf16[1280,2048]{1,0:T(8,128)(2,1)} %all-gather.5.cloned.1.call-done, bf16[1,2048,896]{2,1,0:T(8,128)(2,1)} %param.26), kind=kOutput, calls=%fused_computation.20 | convolution fusion | flops 9404743680 | bytes 22413312 | tf_op jit(solution)/shard_map/dot_general | solution.py:148
  140.3 5.2 %all-to-all-start.2 = ((bf16[4,320,2048]{2,1,0:T(8,128)(2,1)}), bf16[4,320,2048]{2,1,0:T(8,128)(2,1)}, u32[]{:S(2)}, u32[]{:S(2)}) async-start(bf16[4,320,2048]{2,1,0:T(8,128)(2,1)} %bitcast.109), calls=%async_computation.2 | async-start | bytes 10485760 | tf_op jit(solution)/shard_map/all_to_all | solution.py:24
  145.7 59.1 %all-to-all-done.2 = bf16[4,320,2048]{2,1,0:T(8,128)(2,1)} async-done(((bf16[4,320,2048]{2,1,0:T(8,128)(2,1)}), bf16[4,320,2048]{2,1,0:T(8,128)(2,1)}, u32[]{:S(2)}, u32[]{:S(2)}) %all-to-all-start.2) | async-done | bytes 5242912 | tf_op jit(solution)/shard_map/all_to_all | solution.py:24
  204.8 3.6 reduce_sum.92
  208.5 1.5 reshape.143
  210.0 8.8 %all-to-all-start.3 = ((bf16[32,10,2048]{2,1,0:T(8,128)(2,1)}), bf16[32,10,2048]{2,1,0:T(8,128)(2,1)S(1)}, u32[]{:S(2)}, u32[]{:S(2)}) async-start(bf16[32,10,2048]{2,1,0:T(8,128)(2,1)} %reshape.143), calls=%async_computation.3 | async-start | bytes 4194304 | tf_op jit(solution)/shard_map/all_to_all | solution.py:152
  218.8 11.4 %fusion.41 = (bf16[16384,256]{0,1:T(8,128)(2,1)}, bf16[16384,256]{0,1:T(8,128)(2,1)}) fusion(bf16[16384,512]{0,1:T(8,128)(2,1)} %all-gather.3.cloned.1.call-done), kind=kLoop, calls=%fused_computation.71 | loop fusion | bytes 33554432 | tf_op jit(solution)/shard_map/split | solution.py:14
  230.2 98.9 %while.18 = (s32[]{:T(128)}, f32[2,2,512]{2,1,0:T(2,128)S(1)}, f32[2,2,512]{2,1,0:T(2,128)S(1)}, f32[2,2,512,128]{2,3,0,1:T(8,128)}, bf16[16384,256]{0,1:T(8,128...) while((s32[]{:T(128)}, f32[2,2,512]{2,1,0:T(2,128)S(1)}, ...), condition=%wide.region_3.0_spmd.clone, body=%wide.region_0.0_spmd.clone.sunk | while | flops 818685952 | bytes 39198952 | solution.py:95
  231.5 1.3 bitcast_reduce_fusion.2
  232.9 1.6 fusion.68
  239.1 1.6 fusion.68
  243.9 1.3 bitcast_reduce_fusion.2
  245.2 1.6 fusion.68
  251.4 1.6 fusion.68
  256.2 1.3 bitcast_reduce_fusion.2
  257.6 1.6 fusion.68
  262.4 1.3 bitcast_reduce_fusion.2
  263.8 1.6 fusion.68
  268.6 1.3 bitcast_reduce_fusion.2
  269.9 1.6 fusion.68
  274.8 1.3 bitcast_reduce_fusion.2
  276.1 1.6 fusion.68
  280.9 1.3 bitcast_reduce_fusion.2
  282.3 1.6 fusion.68
  288.5 1.6 fusion.68
  293.3 1.3 bitcast_reduce_fusion.2
  294.6 1.6 fusion.68
  300.8 1.6 fusion.68
  305.7 1.3 bitcast_reduce_fusion.2
  307.0 1.6 fusion.68
  313.2 1.6 fusion.68
  318.0 1.3 bitcast_reduce_fusion.2
  319.4 1.6 fusion.68
  325.5 1.6 fusion.68
  329.1 1.4 broadcast_divide_fusion
  330.7 2.2 bitcast_convert_fusion
  332.9 4.4 %all-to-all-start = ((bf16[4,128,2048]{2,1,0:T(8,128)(2,1)}), bf16[4,128,2048]{2,1,0:T(8,128)(2,1)}, u32[]{:S(2)}, u32[]{:S(2)}) async-start(bf16[4,128,2048]{2,1,0:T(8,128)(2,1)} %bitcast.5), calls=%async_computation | async-start | bytes 4194304 | tf_op jit(solution)/shard_map/all_to_all | solution.py:24
  338.0 2.5 reshape.144
  340.5 1.4 gather_fusion
  342.6 4.9 %multiply_reduce_fusion = bf16[128,2048]{1,0:T(8,128)(2,1)} fusion(bf16[128,2,2048]{2,1,0:T(2,128)(2,1)S(1)} %gather.7, pred[128,2]{1,0:T(8,128)(4,1)S(1)} %copy.72, f32[128,2]{1,0:T(8,128)S(1)} %copy.67), kind=kLoop, calls=%fused_computation.28 | loop fusion | flops 1835008 | bytes 1574144 | tf_op jit(solution)/shard_map/reduce_sum | solution.py:162
  347.5 15.9 %all-to-all-done = bf16[4,128,2048]{2,1,0:T(8,128)(2,1)} async-done(((bf16[4,128,2048]{2,1,0:T(8,128)(2,1)}), bf16[4,128,2048]{2,1,0:T(8,128)(2,1)}, u32[]{:S(2)}, u32[]{:S(2)}) %all-to-all-start) | async-done | bytes 2097184 | tf_op jit(solution)/shard_map/all_to_all | solution.py:24
  363.4 2.9 reduce_sum.87
  (227 shorter events, 66.5 us)
Async XLA Ops:
  7.2 323.5 %copy-start = (bf16[256,2048]{1,0:T(8,128)(2,1)S(1)}, bf16[256,2048]{1,0:T(8,128)(2,1)}, u32[]{:S(2)}) copy-start(bf16[256,2048]{1,0:T(8,128)(2,1)} %param.20) | copy-start | bytes 3145732
  7.2 105.2 %all-gather.5.cloned.1.call-start = ((), (), s32[]{:S(2)}) async-start(), calls=%async_computation.5 | async-start | bytes 6553600 | tf_op jit(solution)/shard_map/all_gather | solution.py:133
  16.5 41.6 %copy-start.4 = (bf16[512,256]{1,0:T(8,128)(2,1)S(1)}, bf16[512,256]{1,0:T(8,128)(2,1)}, u32[]{:S(2)}) copy-start(bf16[512,256]{1,0:T(8,128)(2,1)} %param.16) | copy-start | bytes 786436
  54.4 3.9 %copy-start.5 = (bf16[512,256]{1,0:T(8,128)(2,1)S(1)}, bf16[512,256]{1,0:T(8,128)(2,1)}, u32[]{:S(2)}) copy-start(bf16[512,256]{1,0:T(8,128)(2,1)} %param.17) | copy-start | bytes 786436
  58.1 160.7 %all-gather.3.cloned.1.call-start = ((), (), s32[]{:S(2)}) async-start(), calls=%async_computation.4 | async-start | bytes 17301504 | tf_op jit(solution)/shard_map/all_gather | solution.py:13
  140.3 5.2 %copy-start.6 = (bf16[512,256]{1,0:T(8,128)(2,1)S(1)}, bf16[512,256]{1,0:T(8,128)(2,1)}, u32[]{:S(2)}) copy-start(bf16[512,256]{1,0:T(8,128)(2,1)} %param.15) | copy-start | bytes 786436
  140.3 64.5 %all-to-all-start.2 = ((bf16[4,320,2048]{2,1,0:T(8,128)(2,1)}), bf16[4,320,2048]{2,1,0:T(8,128)(2,1)}, u32[]{:S(2)}, u32[]{:S(2)}) async-start(bf16[4,320,2048]{2,1,0:T(8,128)(2,1)} %bitcast.109), calls=%async_computation.2 | async-start | bytes 10485760 | tf_op jit(solution)/shard_map/all_to_all | solution.py:24
  210.0 122.9 %all-to-all-start.3 = ((bf16[32,10,2048]{2,1,0:T(8,128)(2,1)}), bf16[32,10,2048]{2,1,0:T(8,128)(2,1)S(1)}, u32[]{:S(2)}, u32[]{:S(2)}) async-start(bf16[32,10,2048]{2,1,0:T(8,128)(2,1)} %reshape.143), calls=%async_computation.3 | async-start | bytes 4194304 | tf_op jit(solution)/shard_map/all_to_all | solution.py:152
  230.2 100.2 %copy-start.9 = (f32[2]{0:T(128)S(1)}, f32[2]{0:T(128)}, u32[]{:S(2)}) copy-start(f32[2]{0:T(128)} %param.18) | copy-start | bytes 28
  230.2 100.5 %copy-start.10 = (f32[128]{0:T(128)S(1)}, f32[128]{0:T(128)}, u32[]{:S(2)}) copy-start(f32[128]{0:T(128)} %param.19) | copy-start | bytes 1540
  232.9 1.7 copy-start.2
  235.5 1.0 copy-start.3
  239.0 1.7 copy-start.2
  241.6 1.0 copy-start.3
  245.2 1.7 copy-start.2
  247.8 1.0 copy-start.3
  251.4 1.7 copy-start.2
  254.0 1.0 copy-start.3
  257.6 1.7 copy-start.2
  260.2 1.0 copy-start.3
  263.7 1.7 copy-start.2
  266.3 1.0 copy-start.3
  269.9 1.7 copy-start.2
  272.5 1.0 copy-start.3
  276.1 1.7 copy-start.2
  278.7 1.0 copy-start.3
  282.3 1.7 copy-start.2
  284.9 1.0 copy-start.3
  288.5 1.7 copy-start.2
  291.1 1.0 copy-start.3
  294.6 1.7 copy-start.2
  297.2 1.0 copy-start.3
  300.8 1.7 copy-start.2
  303.4 1.0 copy-start.3
  307.0 1.7 copy-start.2
  309.6 1.0 copy-start.3
  313.2 1.7 copy-start.2
  315.8 1.0 copy-start.3
  319.3 1.7 copy-start.2
  321.9 1.0 copy-start.3
  325.5 1.7 copy-start.2
  328.1 1.0 copy-start.3
  330.5 6.9 %copy-start.7 = (s32[128,2]{0,1:T(2,128)S(1)}, s32[128,2]{0,1:T(2,128)}, u32[]{:S(2)}) copy-start(s32[128,2]{0,1:T(2,128)} %param.23) | copy-start | bytes 3076
  330.5 7.2 %copy-start.8 = (f32[128,2]{0,1:T(2,128)S(1)}, f32[128,2]{0,1:T(2,128)}, u32[]{:S(2)}) copy-start(f32[128,2]{0,1:T(2,128)} %param.24) | copy-start | bytes 3076
  332.9 5.1 %copy-start.1 = (bf16[32,10,2048]{2,1,0:T(8,128)(2,1)}, bf16[32,10,2048]{2,1,0:T(8,128)(2,1)S(1)}, u32[]{:S(2)}) copy-start(bf16[32,10,2048]{2,1,0:T(8,128)(2,1)S(1)} %all-to-all-done.3) | copy-start | bytes 3932164
  332.9 30.5 %all-to-all-start = ((bf16[4,128,2048]{2,1,0:T(8,128)(2,1)}), bf16[4,128,2048]{2,1,0:T(8,128)(2,1)}, u32[]{:S(2)}, u32[]{:S(2)}) async-start(bf16[4,128,2048]{2,1,0:T(8,128)(2,1)} %bitcast.5), calls=%async_computation | async-start | bytes 4194304 | tf_op jit(solution)/shard_map/all_to_all | solution.py:24
Sparse Core Ops, SparseCore 0:
  58.2 54.1 all-gather.4
  115.2 81.1 all-gather.2
where the time goes:
time: 374 us; the launch traced here: 373 us
  waiting for transfers between devices  128 us (34%)
  matrix products  68.6 us (18%)
  local copies, waits for them, and re-layouts  62.1 us (17%)
  other arithmetic  42.4 us (11%)
  blocking collectives  37.9 us (10%)
  starting transfers between devices  18.5 us (5%)
  between operations  14.3 us (4%)
    all_to_all x2, waiting for transfers between devices, summed_on_arrival(): lax.all_to_all(split_up(array, dim, devices), axis, 0, 0, tiled=True)  75 us
    all_gather x1, waiting for transfers between devices, per_device(): lax.all_gather(arrived.reshape(experts_all * slot_count, model_width), 't...  53.1 us
    all_to_all x1, blocking collectives, per_device(): lax.all_to_all(outgoing, 'ep', split_axis=0, concat_axis=0, tiled=True)  37.9 us
    convert_element_type x16, other arithmetic, attend_block(): weights.astype(jnp.bfloat16)  25.2 us
    dot_general x16, matrix products, attend_block(): jnp.einsum('qhid,khid->ihqk', query_maps, key_maps, preferred_element_typ...  21 us
    dynamic_slice x16, local copies, waits for them, and re-layouts, loop_body(): lax.dynamic_slice_in_dim(value_piece, first_row, block_rows, 0)  20.3 us
    dot_general x1, matrix products, per_device(): jnp.dot(hidden, down_local, preferred_element_type=jnp.float32)  17.9 us
    while x80, local copies, waits for them, and re-layouts  15.6 us
  transfers between devices with their start and end apart: 5, of which 3 were waited for; matrix products, arithmetic and copies ran while one was open for 38% of the time, Pallas kernels for 0%

commit v1 on v0

v1 whole, which is shorter than its diff:
```python
import functools
import jax
import jax.numpy as jnp
from jax import lax
from jax.experimental import pallas as pl
from jax.experimental.pallas import tpu as pltpu
from jax.sharding import PartitionSpec as P

F32 = jnp.float32
BF = jnp.bfloat16
epsilon = 1e-06
init_lambda = 0.2
LIM = 100.0
LOG2E = 1.4426950408889634
def attn_kernel(q_ref, kv_ref, o_ref, st_ref, acc_ref, *, nq, nblk, kb, qt):
    lane_id = lax.broadcasted_iota(jnp.int32, (256, 128), 0) // 64
    pick = (lane_id == lax.broadcasted_iota(jnp.int32, (256, 128), 1)).astype(BF)
    def norms(b, best):
        k = kv_ref[b, :kb, :].astype(F32)
        kk = jnp.dot((k * k).astype(BF), pick, preferred_element_type=F32)
        return jnp.maximum(best, jnp.max(kk, axis=0, keepdims=True))
    kmax = lax.fori_loop(0, nblk, norms, jnp.zeros((1, 128), F32))
    qf = q_ref[...].astype(F32)
    qq = jnp.sum((qf * qf).reshape(4, 64, nq), axis=1)
    bound2 = jnp.max(qq) * jnp.max(kmax) * (LOG2E * LOG2E * 1.05)
    small = bound2 < LIM * LIM
    row = lax.broadcasted_iota(jnp.int32, (128, 1), 0)
    ones = jnp.ones((16, 256), BF)

    def head_queries(h, i):
        qh = q_ref[128 * h:128 * h + 128, :]
        return jnp.where((row // 64) == i, qh, jnp.zeros_like(qh))

    @pl.when(small)
    def _():
        for h in range(2):
            qs = [head_queries(h, i) for i in range(2)]
            acc_ref[...] = jnp.zeros_like(acc_ref)
            def body(b, _):
                kh = kv_ref[b, :kb, 128 * h:128 * h + 128]
                vts = [jnp.concatenate([kv_ref[b, kb + 256 * t + 128 * h: kb + 256 * t + 128 * h + 128, :], ones], 0) for t in range(kb // 256)]
                for i in range(2):
                    for j in range(nq // qt):
                        s = jnp.dot(kh, qs[i][:, j * qt:(j + 1) * qt], preferred_element_type=F32)
                        p = jnp.exp2(s * LOG2E).astype(BF)
                        add = sum(jnp.dot(vts[t], p[256 * t:256 * t + 256], preferred_element_type=F32) for t in range(kb // 256))
                        acc_ref[i, :, j * qt:(j + 1) * qt] += add
                return 0
            lax.fori_loop(0, nblk, body, 0)
            for i in range(2):
                o_ref[2 * h + i] = acc_ref[i, :128]
                st_ref[2 * h + i] = acc_ref[i, 128:136]
                st_ref[4 + 2 * h + i] = jnp.zeros((8, nq), F32)

    @pl.when(jnp.logical_not(small))
    def _():
        for h in range(2):
            for i in range(2):
                qi = head_queries(h, i)
                for j in range(nq // qt):
                    acc_ref[i, :, j * qt:(j + 1) * qt] = jnp.zeros((144, qt), F32)
                    def body(b, m):
                        kh = kv_ref[b, :kb, 128 * h:128 * h + 128]
                        s = jnp.dot(kh, qi[:, j * qt:(j + 1) * qt], preferred_element_type=F32)
                        mn = jnp.maximum(m, jnp.max(s, axis=0, keepdims=True))
                        p = jnp.exp2((s - mn) * LOG2E).astype(BF)
                        add = 0.0
                        for t in range(kb // 256):
                            vt = jnp.concatenate([kv_ref[b, kb + 256 * t + 128 * h: kb + 256 * t + 128 * h + 128, :], ones], 0)
                            add = add + jnp.dot(vt, p[256 * t:256 * t + 256], preferred_element_type=F32)
                        acc_ref[i, :, j * qt:(j + 1) * qt] = acc_ref[i, :, j * qt:(j + 1) * qt] * jnp.exp2((m - mn) * LOG2E) + add
                        return mn
                    m = lax.fori_loop(0, nblk, body, jnp.full((1, qt), -1e30, F32))
                    sl = slice(j * qt, (j + 1) * qt)
                    o_ref[2 * h + i, :, sl] = acc_ref[i, :128, sl]
                    st_ref[2 * h + i, :, sl] = acc_ref[i, 128:136, sl]
                    st_ref[4 + 2 * h + i, :, sl] = jnp.broadcast_to(m, (8, qt))

def attention(qT, kv, qt=1024):
    nq = qT.shape[1]; nblk, kb2, _ = kv.shape; kb = kb2 // 2
    return pl.pallas_call(
        functools.partial(attn_kernel, nq=nq, nblk=nblk, kb=kb, qt=qt),
        out_shape=(jax.ShapeDtypeStruct((4, 128, nq), F32), jax.ShapeDtypeStruct((8, 8, nq), F32)),
        in_specs=[pl.BlockSpec(memory_space=pltpu.VMEM)] * 2,
        out_specs=(pl.BlockSpec(memory_space=pltpu.VMEM),) * 2,
        scratch_shapes=[pltpu.VMEM((2, 144, nq), F32)],
        compiler_params=pltpu.CompilerParams(vmem_limit_bytes=40 * 2**20),
        cost_estimate=pl.CostEstimate(flops=4 * nblk * kb * nq * 4 * 192 // 2, bytes_accessed=16 * 2**20, transcendentals=4 * nblk * kb * nq),
        name="attention",
    )(qT, kv)


def attend(queries, key_rows, value_rows, lambdas, head_gain):
    rows = queries.shape[0]
    n = lax.axis_size("ep")
    keys_t = value_rows.T
    packed = jnp.concatenate([key_rows, keys_t[:, :256], keys_t[:, 256:]], axis=0)
    groups = [[2 * k + c for k in range(n // 2)] for c in range(2)]
    kv = lax.all_gather(packed, "ep", axis_index_groups=groups, axis=0, tiled=True)
    kv = kv.reshape(n // 2, 2 * rows, 256)
    swap = [(k, k ^ 1) for k in range(n)]
    mine = (queries * jnp.asarray(0.125, BF)).T
    other = lax.ppermute(mine, "ep", swap)
    out, stats = attention(jnp.concatenate([mine, other], axis=1), kv)
    stats = stats[:, 0]
    far_out = lax.ppermute(out[:, :, rows:], "ep", swap)
    far_stats = lax.ppermute(stats[:, rows:], "ep", swap)
    near_max, far_max = stats[4:, :rows], far_stats[4:]
    top = jnp.maximum(near_max, far_max)
    near, far = jnp.exp(near_max - top), jnp.exp(far_max - top)
    totals = stats[:4, :rows] * near + far_stats[:4] * far
    maps = (out[:, :, :rows] * near[:, None] + far_out * far[:, None]) / totals[:, None]
    head_out = maps[0::2] - lambdas[:, None, None] * maps[1::2]
    mean_square = jnp.mean(head_out * head_out, axis=1, keepdims=True)
    attended = head_out * lax.rsqrt(mean_square + epsilon) * head_gain[:, None] * (1.0 - init_lambda)
    return attended.astype(BF).reshape(256, rows)


def capacity(tokens, top_count, experts):
    return max(2, (top_count * tokens * 5 + 4 * experts - 1) // (4 * experts))


def per_device(
    queries, key_rows, value_rows, lambdas, head_gain, out_weight, moe_input, moe_gain,
    routes, route_logits, expert_gate, expert_up, expert_down,
):
    model_width = out_weight.shape[1]
    attended = attend(queries, key_rows, value_rows, lambdas, head_gain)
    token_count, top_count = routes.shape
    experts_all = lax.axis_size("ep")
    slot_count = capacity(token_count, top_count, experts_all)
    moe_float = moe_input.astype(F32)
    normed = (
        moe_float
        * lax.rsqrt(jnp.mean(moe_float * moe_float, axis=-1, keepdims=True) + epsilon)
        * moe_gain
    ).astype(BF)
    gate_weights = jax.nn.softmax(route_logits, axis=-1)
    flat_routes = routes.reshape(-1)
    chosen = (flat_routes[:, None] == jnp.arange(experts_all, dtype=jnp.int32)[None, :]).astype(jnp.int32)
    slot_rank = jnp.sum((jnp.cumsum(chosen, axis=0) - chosen) * chosen, axis=1)
    slot_ids = (flat_routes * slot_count + slot_rank).reshape(token_count, top_count)
    dispatch = jnp.any(
        slot_ids[None, :, :] == jnp.arange(experts_all * slot_count, dtype=jnp.int32)[:, None, None],
        axis=-1,
    ).astype(BF)
    outgoing = jnp.dot(dispatch, normed, preferred_element_type=F32).astype(BF)
    arrived = lax.all_to_all(outgoing, "ep", split_axis=0, concat_axis=0, tiled=True)
    segment = lax.all_gather(arrived, "tp", axis=0, tiled=True)
    gate_part = jnp.dot(segment, expert_gate[0], preferred_element_type=F32)
    up_part = jnp.dot(segment, expert_up[0], preferred_element_type=F32)
    hidden = (jax.nn.silu(gate_part) * up_part).astype(BF)
    expert_part = jnp.dot(hidden, expert_down[0], preferred_element_type=F32).astype(BF)
    reply = lax.psum_scatter(expert_part, "tp", scatter_dimension=0, tiled=True)
    replies = lax.all_to_all(reply, "ep", split_axis=0, concat_axis=0, tiled=True)
    weights = jnp.sum(
        jnp.where(
            slot_ids[:, :, None] == jnp.arange(experts_all * slot_count, dtype=jnp.int32),
            gate_weights[:, :, None],
            0.0,
        ),
        axis=1,
    )
    picked = jnp.take(replies, slot_ids.reshape(-1), axis=0).reshape(token_count, top_count, model_width)
    expert_out = jnp.sum(gate_weights[:, :, None] * picked.astype(F32), axis=1).astype(BF)
    mixer_part = lax.dot_general(
        attended, out_weight, (((0,), (0,)), ((), ())), preferred_element_type=F32
    ).astype(BF)
    mixer_out = lax.psum_scatter(mixer_part, "tp", scatter_dimension=0, tiled=True)
    return (mixer_out, expert_out)


def solution(mesh):
    placed = (
        P("ep", "tp"),
        P("ep", "tp"),
        P("ep", "tp"),
        P("tp"),
        P(),
        P("tp", None),
        P(("ep", "tp"), None),
        P(),
        P(("ep", "tp"), None),
        P(("ep", "tp"), None),
        P("ep", None, "tp"),
        P("ep", None, "tp"),
        P("ep", "tp", None),
    )
    return jax.shard_map(
        per_device,
        mesh=mesh,
        in_specs=placed,
        out_specs=(P(("ep", "tp"), None), P(("ep", "tp"), None)),
        check_vma=False,
    )
```

time: 374 us -> 319 us (0.85)
  Pallas kernels: 0 us -> 67.7 us
  local copies, waits for them, and re-layouts: 62.1 us -> 20.7 us
  matrix products: 68.6 us -> 32.7 us
  other arithmetic: 42.4 us -> 9.26 us
  starting transfers between devices: 18.5 us -> 7.92 us
    pallas_call x0 -> x1, Pallas kernels: none -> 67.7 us  [attention(): pl.pallas_call(functools.partial(attn_kernel, nq=nq, nblk=nblk, kb=kb, qt...]
    all_to_all x3 -> x1, waiting for transfers between devices: 75 us -> 28.1 us  [per_device(): lax.all_to_all(reply, 'ep', split_axis=0, concat_axis=0, tiled=True)]
    all_gather x2, waiting for transfers between devices: 53.1 us -> 96.1 us  [the longest x1 53.1 us: per_device(): segment = lax.all_gather(arrived, 'tp', axis=0, tiled=True)]
    dot_general x36 -> x4, matrix products: 68.6 us -> 32.7 us  [the longest x1 17.9 us: per_device(): jnp.dot(hidden, expert_down[0], preferred_element_type=F32).astype(BF)]
    convert_element_type x16 -> x1, other arithmetic: 25.2 us -> 0.16 us  [attend(): return attended.astype(BF).reshape(256, rows)]
    dynamic_slice x16 -> x0, local copies, waits for them, and re-layouts: 20.3 us -> none  [loop_body(): lax.dynamic_slice_in_dim(value_piece, first_row, block_rows, 0)]
    while x81 -> x0, local copies, waits for them, and re-layouts: 15.6 us -> none
    all_to_all x3 -> x1, starting transfers between devices: 18.4 us -> 5.76 us  [per_device(): lax.all_to_all(reply, 'ep', split_axis=0, concat_axis=0, tiled=True)]
  transfers between devices with their start and end apart: 5 -> 8, of which waited for: 3 -> 5; matrix products, arithmetic and copies ran while one was open for 38% -> 12% of each run, Pallas kernels for 0% -> 21%
where the time goes in v1:
time: 319 us; the launch traced here: 318 us
  waiting for transfers between devices  128 us (40%)
  Pallas kernels  67.7 us (21%)
  blocking collectives  37.9 us (12%)
  matrix products  32.7 us (10%)
  local copies, waits for them, and re-layouts  20.7 us (6%)
  between operations  14.1 us (4%)
  other arithmetic  9.26 us (3%)
  starting transfers between devices  7.92 us (2%)
    pallas_call x1, Pallas kernels, attention(): pl.pallas_call(functools.partial(attn_kernel, nq=nq, nblk=nblk, kb=kb, qt...  67.7 us
    all_gather x1, waiting for transfers between devices, per_device(): segment = lax.all_gather(arrived, 'tp', axis=0, tiled=True)  53.1 us
    all_gather x1, waiting for transfers between devices, attend(): lax.all_gather(packed, 'ep', axis_index_groups=groups, axis=0, tiled=True)  42.9 us
    all_to_all x1, blocking collectives, per_device(): lax.all_to_all(outgoing, 'ep', split_axis=0, concat_axis=0, tiled=True)  37.9 us
    all_to_all x1, waiting for transfers between devices, per_device(): lax.all_to_all(reply, 'ep', split_axis=0, concat_axis=0, tiled=True)  28.1 us
    dot_general x1, matrix products, per_device(): jnp.dot(hidden, expert_down[0], preferred_element_type=F32).astype(BF)  17.9 us
    dot_general x1, matrix products, per_device(): gate_part = jnp.dot(segment, expert_gate[0], preferred_element_type=F32)  9.98 us
  transfers between devices with their start and end apart: 8, of which 5 were waited for; matrix products, arithmetic and copies ran while one was open for 12% of the time, Pallas kernels for 21%

profile of v1, /device:TPU:1, one launch (start us, length us, event | category | flops | bytes accessed | tf_op | source)
XLA Modules:
  0.0 317.8 jit_solution(339664573911919854)
XLA Ops:
  7.2 0.9 copy.42
  8.1 0.1 eq.39
  8.2 0.1 reshape.109
  8.4 0.6 reduce-window.6
  9.0 0.2 slice_reduce_fusion
  9.2 0.1 fusion.13
  9.3 0.1 reduce_sum.52
  9.5 0.1 copy.45
  9.5 0.7 compare_and_fusion
  10.3 1.2 fusion.4
  11.5 2.7 convolution_convert_fusion.2
  14.2 2.3 all_to_all.16
  16.5 37.9 %all_to_all.24 = bf16[32,10,2048]{2,1,0:T(8,128)(2,1)} all-to-all(bf16[32,10,2048]{2,1,0:T(8,128)(2,1)S(1)} %all_to_all.16), channel_id=1, replica_groups=mesh['ep'=32,'tp'=4] {'ep'}, dimensions={0} | all-to-all | bytes 2621440 | tf_op jit(solution)/shard_map/all_to_all | solution.py:148
  54.4 3.6 %all_to_all.18 = bf16[320,2048]{1,0:T(8,128)(2,1)} reshape(bf16[32,10,2048]{2,1,0:T(8,128)(2,1)} %all_to_all.24) | data formatting | bytes 2621440 | tf_op jit(solution)/shard_map/all_to_all | solution.py:148
  58.2 0.1 copy.39
  58.3 0.1 copy.40
  58.4 0.8 pad_maximum_fusion.1
  59.3 0.0 reduce-scatter.5.cloned.1.call-start
  59.3 53.1 %all-gather.5.cloned.1.call-done = bf16[1280,2048]{1,0:T(8,128)(2,1)} async-done(((bf16[320,2048]{1,0:T(8,128)(2,1)}), bf16[1280,2048]{1,0:T(8,128)(2,1)}) %all-gather.5.cloned.1.call-update) | async-done | bytes 5242896 | tf_op jit(solution)/shard_map/all_gather | solution.py:149
  112.4 10.0 %fusion.2 = f32[1280,896]{1,0:T(8,128)} fusion(bf16[1280,2048]{1,0:T(8,128)(2,1)} %all-gather.5.cloned.1.call-done, bf16[1,2048,896]{2,1,0:T(8,128)(2,1)} %param.23), kind=kOutput, calls=%fused_computation.5 | convolution fusion | flops 4697620480 | bytes 13500416 | tf_op jit(solution)/shard_map/dot_general | solution.py:150
  122.4 17.9 %convolution_convert_fusion = bf16[1280,2048]{1,0:T(8,128)(2,1)} fusion(bf16[1,896,2048]{2,1,0:T(8,128)(2,1)} %param.25, f32[1280,896]{1,0:T(8,128)} %fusion.2, bf16[1280,2048]{1,0:T(8,128)(2,1)} %all-gather.5.cloned.1.call-done, bf16[1,2048,896]{2,1,0:T(8,128)(2,1)} %param.24), kind=kOutput, calls=%fused_computation.1 | convolution fusion | flops 9404743680 | bytes 22413312 | tf_op jit(solution)/shard_map/dot_general | solution.py:153
  140.4 0.9 copy-done.3
  141.3 0.1 copy.38
  141.5 1.0 collective-permute-start
  142.5 1.2 collective-permute-done
  143.6 0.1 pad_maximum_fusion.q_ref
  143.7 42.9 %all-gather.3.cloned.1.call-done = bf16[16384,256]{1,0:T(8,128)(2,1)} async-done(((bf16[1024,256]{1,0:T(8,128)(2,1)}), bf16[16384,256]{1,0:T(8,128)(2,1)}) %all-gather.3.cloned.1.call-update) | async-done | bytes 8388624 | tf_op jit(solution)/shard_map/all_gather | solution.py:99
  186.6 3.4 %copy-done.1 = bf16[16384,256]{1,0:T(8,128)(2,1)S(1)} copy-done((bf16[16384,256]{1,0:T(8,128)(2,1)S(1)}, bf16[16384,256]{1,0:T(8,128)(2,1)}, u32[]{:S(2)}) %copy-start.1) | copy-done | bytes 8388632
  190.0 67.7 %attention.1 = (f32[4,128,1024]{2,1,0:T(8,128)S(1)}, f32[8,8,1024]{2,1,0:T(8,128)S(1)}) custom-call(bf16[256,1024]{1,0:T(8,128)(2,1)S(1)} %pad_maximum_fusion.q_ref, bf16[16,1024,256]{2,1,0:T(8,128)(2,1)S(1)} %bitcast.52), custom_call_target="tpu_custom_call" | custom-call | flops 12884901888 | bytes 16777216 | tf_op jit(solution)/shard_map/attention/pallas_call | solution.py:81
  257.7 0.1 slice.49
  257.8 0.9 collective-permute-start.2
  258.8 0.1 collective-permute-start.1
  258.9 2.2 collective-permute-done.1
  261.1 0.3 add_divide_fusion
  261.3 0.2 multiply_reduce_fusion.1
  261.5 0.2 multiply_convert_fusion.1
  261.7 2.1 convolution_convert_fusion.1
  263.9 3.4 %all_to_all.19 = bf16[32,10,2048]{2,1,0:T(8,128)(2,1)} reshape(bf16[320,2048]{1,0:T(8,128)(2,1)} %reduce-scatter.5.cloned.1.call-done) | data formatting | bytes 2621440 | tf_op jit(solution)/shard_map/all_to_all | solution.py:155
  267.3 5.8 %all-to-all-start.1 = ((bf16[32,10,2048]{2,1,0:T(8,128)(2,1)}), bf16[32,10,2048]{2,1,0:T(8,128)(2,1)}, u32[]{:S(2)}, u32[]{:S(2)}) async-start(bf16[32,10,2048]{2,1,0:T(8,128)(2,1)} %all_to_all.19), calls=%async_computation.3 | async-start | bytes 4194304 | tf_op jit(solution)/shard_map/all_to_all | solution.py:155
  273.1 0.1 copy.47
  273.2 0.1 mul.147
  273.3 0.1 copy.46
  273.5 0.1 copy.41
  273.7 28.1 %all-to-all-done.1 = bf16[32,10,2048]{2,1,0:T(8,128)(2,1)} async-done(((bf16[32,10,2048]{2,1,0:T(8,128)(2,1)}), bf16[32,10,2048]{2,1,0:T(8,128)(2,1)}, u32[]{:S(2)}, u32[]{:S(2)}) %all-to-all-start.1) | async-done | bytes 1310752 | tf_op jit(solution)/shard_map/all_to_all | solution.py:155
  301.8 2.5 all_to_all.21
  304.3 1.4 gather_fusion
  305.6 0.7 gather.7
  306.4 4.9 %multiply_reduce_fusion = bf16[128,2048]{1,0:T(8,128)(2,1)} fusion(bf16[128,2,2048]{2,1,0:T(2,128)(2,1)S(1)} %gather.7, pred[128,2]{1,0:T(8,128)(4,1)S(1)} %copy.46, f32[128,2]{1,0:T(8,128)S(1)} %copy.41), kind=kLoop, calls=%fused_computation.9 | loop fusion | flops 1835008 | bytes 1574144 | tf_op jit(solution)/shard_map/reduce_sum | solution.py:165
  (44 shorter events, 0.5 us)
Async XLA Ops:
  7.2 254.6 %copy-start = (bf16[256,2048]{1,0:T(8,128)(2,1)S(1)}, bf16[256,2048]{1,0:T(8,128)(2,1)}, u32[]{:S(2)}) copy-start(bf16[256,2048]{1,0:T(8,128)(2,1)} %param.18) | copy-start | bytes 3145732
  7.2 105.3 %all-gather.5.cloned.1.call-start = ((), (), s32[]{:S(2)}) async-start(), calls=%async_computation.6 | async-start | bytes 6553600 | tf_op jit(solution)/shard_map/all_gather | solution.py:149
  16.5 41.6 %copy-start.2 = (bf16[512,256]{1,0:T(8,128)(2,1)S(1)}, bf16[512,256]{1,0:T(8,128)(2,1)}, u32[]{:S(2)}) copy-start(bf16[512,256]{1,0:T(8,128)(2,1)} %param.15) | copy-start | bytes 786436
  54.4 4.0 %copy-start.4 = (bf16[512,256]{1,0:T(8,128)(2,1)S(1)}, bf16[512,256]{1,0:T(8,128)(2,1)}, u32[]{:S(2)}) copy-start(bf16[512,256]{1,0:T(8,128)(2,1)} %param.14) | copy-start | bytes 786436
  58.1 128.5 %all-gather.3.cloned.1.call-start = ((), (), s32[]{:S(2)}) async-start(), calls=%async_computation.4 | async-start | bytes 8912896 | tf_op jit(solution)/shard_map/all_gather | solution.py:99
  59.3 204.6 %reduce-scatter.5.cloned.1.call-start = ((), (), s32[]{:S(2)}) async-start(), calls=%async_computation.7 | async-start | bytes 6553600 | tf_op jit(solution)/shard_map/reduce_scatter | solution.py:154
  140.4 0.9 copy-start.3
  140.4 170.9 %reduce-scatter.3.cloned.1.call-start = ((), (), s32[]{:S(2)}) async-start(), calls=%async_computation.5 | async-start | bytes 2621440 | tf_op jit(solution)/shard_map/reduce_scatter | solution.py:169
  141.5 2.1 collective-permute-start
  186.6 3.4 %copy-start.1 = (bf16[16384,256]{1,0:T(8,128)(2,1)S(1)}, bf16[16384,256]{1,0:T(8,128)(2,1)}, u32[]{:S(2)}) copy-start(bf16[16384,256]{1,0:T(8,128)(2,1)} %all-gather.3.cloned.1.call-done) | copy-start | bytes 25165828
  257.7 3.6 %copy-start.7 = (f32[2]{0:T(128)S(1)}, f32[2]{0:T(128)}, u32[]{:S(2)}) copy-start(f32[2]{0:T(128)} %param.16) | copy-start | bytes 28
  257.7 3.8 %copy-start.8 = (f32[128]{0:T(128)S(1)}, f32[128]{0:T(128)}, u32[]{:S(2)}) copy-start(f32[128]{0:T(128)} %param.17) | copy-start | bytes 1540
  257.8 3.2 %collective-permute-start.2 = (f32[4,128,512]{2,1,0:T(8,128)S(1)}, f32[4,128,512]{2,1,0:T(8,128)S(1)}, u32[]{:S(2)}, u32[]{:S(2)}) collective-permute-start(f32[4,128,512]{2,1,0:T(8,128)S(1)} %slice.49), channel_id=1, source_target_pairs={{0,4},{4,0},{8,12},{12,8},{16,20},{20,16},{24,28},{28,24},{32,36},... | collective-permute-start | bytes 3145736 | tf_op jit(solution)/shard_map/ppermute | solution.py:106
  258.8 2.3 collective-permute-start.1
  263.9 9.2 %copy-start.5 = (s32[128,2]{0,1:T(2,128)S(1)}, s32[128,2]{0,1:T(2,128)}, u32[]{:S(2)}) copy-start(s32[128,2]{0,1:T(2,128)} %param.21) | copy-start | bytes 3076
  263.9 9.6 %copy-start.6 = (f32[128,2]{0,1:T(2,128)S(1)}, f32[128,2]{0,1:T(2,128)}, u32[]{:S(2)}) copy-start(f32[128,2]{0,1:T(2,128)} %param.22) | copy-start | bytes 3076
  267.3 34.5 %all-to-all-start.1 = ((bf16[32,10,2048]{2,1,0:T(8,128)(2,1)}), bf16[32,10,2048]{2,1,0:T(8,128)(2,1)}, u32[]{:S(2)}, u32[]{:S(2)}) async-start(bf16[32,10,2048]{2,1,0:T(8,128)(2,1)} %all_to_all.19), calls=%async_computation.3 | async-start | bytes 4194304 | tf_op jit(solution)/shard_map/all_to_all | solution.py:155
Sparse Core Ops, SparseCore 0:
  58.2 54.1 all-gather.4
  115.1 71.4 all-gather.2
  189.0 55.0 reduce-scatter.4
  264.0 28.8 reduce-scatter.2

commit v2 on v1

--- a/solution.py
+++ b/solution.py
@@ -116,19 +116,221 @@
     return attended.astype(BF).reshape(256, rows)
 
 
-def capacity(tokens, top_count, experts):
-    return max(2, (top_count * tokens * 5 + 4 * experts - 1) // (4 * experts))
+MESH = pl.DeviceIdType.MESH
+GROUPS = 8
+MAIN = 8
+
+
+def front_kernel(
+    main_ref, tail_ref, gate_ref, up_ref, down_ref, out_ref, seg_ref, end_ref, g_buf, u_buf, d_buf,
+    own_sem, load_sem, put_send, put_recv, near_send, near_recv, far_send, far_recv,
+):
+    e, x = lax.axis_index("ep"), lax.axis_index("tp")
+    n = main_ref.shape[0]
+    width = main_ref.shape[2]
+    per = n // GROUPS
+    right, left = lax.rem(x + 1, 4), lax.rem(x + 3, 4)
+    across = lax.rem(x + 2, 4)
+    barrier = pltpu.get_barrier_semaphore()
+
+    def greet(k, _):
+        pl.semaphore_signal(barrier, inc=1, device_id=(e ^ k, x), device_id_type=MESH)
+        return 0
+
+    lax.fori_loop(1, n, greet, 0)
+    for peer in (right, left, across):
+        pl.semaphore_signal(barrier, inc=1, device_id=(e, peer), device_id_type=MESH)
+    pl.semaphore_wait(barrier, n + 2)
+
+    pairs = ((main_ref, seg_ref), (tail_ref, end_ref))
+    own = [pltpu.make_async_copy(src.at[0], dst.at[x, 0], own_sem.at[w]) for w, (src, dst) in enumerate(pairs)]
+    for c in own:
+        c.start()
+    for g in range(GROUPS):
+        def put(k, _, g=g):
+            for w, (src, dst) in enumerate(pairs):
+                pltpu.make_async_remote_copy(
+                    src_ref=src.at[k], dst_ref=dst.at[x, k], send_sem=put_send.at[w], recv_sem=put_recv.at[w, g],
+                    device_id=(e ^ k, x), device_id_type=MESH,
+                ).start()
+            return 0
+
+        lax.fori_loop(max(1, g * per), g * per + per, put, 0)
+    loads = [
+        pltpu.make_async_copy(src, dst, load_sem.at[k])
+        for k, (src, dst) in enumerate(((gate_ref, g_buf), (up_ref, u_buf), (down_ref, d_buf)))
+    ]
+    for c in loads:
+        c.start()
+    for c in own:
+        c.wait()
+
+    def span(g):
+        return pl.ds(g * per, per)
+
+    def near(w, g, d):
+        part = pairs[w][1].at[x, span(g)]
+        return pltpu.make_async_remote_copy(
+            src_ref=part, dst_ref=part, send_sem=near_send.at[w, d, g], recv_sem=near_recv.at[w, d, g],
+            device_id=(e, right if d == 0 else left), device_id_type=MESH,
+        )
+
+    def came(w, g, d):
+        part = pairs[w][1].at[left if d == 0 else right, span(g)]
+        return pltpu.make_async_copy(part, part, near_recv.at[w, d, g])
+
+    def far(w, g):
+        d = g % 2
+        part = pairs[w][1].at[left if d == 0 else right, span(g)]
+        return pltpu.make_async_remote_copy(
+            src_ref=part, dst_ref=part, send_sem=far_send.at[w, g], recv_sem=far_recv.at[w, g],
+            device_id=(e, right if d == 0 else left), device_id_type=MESH,
+        )
+
+    def relay(g):
+        for w in range(2):
+            came(w, g, g % 2).wait()
+            far(w, g).start()
+
+    for g in range(GROUPS):
+        first = 1 if g == 0 else g * per
+        for w, (src, dst) in enumerate(pairs):
+            landed = dst.at[x, pl.ds(first, g * per + per - first)]
+            pltpu.make_async_copy(landed, landed, put_recv.at[w, g]).wait()
+        for w in range(2):
+            for d in range(2):
+                near(w, g, d).start()
+        if g >= 3:
+            relay(g - 3)
+    for c in loads:
+        c.wait()
+
+    def expert(t, _):
+        @pl.when(t == 1)
+        def _():
+            for g in range(GROUPS - 3, GROUPS):
+                relay(g)
+            for w in range(2):
+                for g in range(0, GROUPS, 2):
+                    came(w, g, 1).wait()
+
+        @pl.when(t == 2)
+        def _():
+            for w in range(2):
+                for g in range(1, GROUPS, 2):
+                    came(w, g, 0).wait()
+
+        @pl.when(t == 3)
+        def _():
+            for w in range(2):
+                for g in range(GROUPS):
+                    part = pairs[w][1].at[across, span(g)]
+                    pltpu.make_async_copy(part, part, far_recv.at[w, g]).wait()
+
+        j = lax.rem(x + turn(t), 4)
+        rows = jnp.concatenate(
+            [seg_ref[j].reshape(n * MAIN, width), end_ref[j].reshape(n * 2, width)], axis=0
+        )
+        gate = jnp.dot(rows, g_buf[...], preferred_element_type=F32)
+        up = jnp.dot(rows, u_buf[...], preferred_element_type=F32)
+        hidden = (gate / (1.0 + jnp.exp(-gate)) * up).astype(BF)
+        out_ref[j] = jnp.dot(hidden, d_buf[...], preferred_element_type=F32).astype(BF)
+        return 0
+
+    lax.fori_loop(0, 4, expert, 0)
+    for w, (src, dst) in enumerate(pairs):
+        sent = dst.at[x, pl.ds(1, n - 1)]
+        pltpu.make_async_copy(sent, sent, put_send.at[w]).wait()
+        for g in range(GROUPS):
+            for d in range(2):
+                near(w, g, d).wait_send()
+            far(w, g).wait_send()
+
+
+def turn(t):
+    return t + (t // 2) * (1 - 2 * (t % 2))
+
+
+def front(main, tail, gate, up, down):
+    n, _, width = main.shape
+    dma = pltpu.SemaphoreType.DMA
+    hbm = pl.BlockSpec(memory_space=pl.ANY)
+    return pl.pallas_call(
+        front_kernel,
+        out_shape=jax.ShapeDtypeStruct((4, n * (MAIN + 2), width), BF),
+        in_specs=[hbm] * 5,
+        out_specs=pl.BlockSpec(memory_space=pltpu.VMEM),
+        scratch_shapes=[
+            pltpu.VMEM((4, n, MAIN, width), BF), pltpu.VMEM((4, n, 2, width), BF),
+            pltpu.VMEM(gate.shape, BF), pltpu.VMEM(up.shape, BF), pltpu.VMEM(down.shape, BF),
+            dma((2,)), dma((3,)), dma((2,)), dma((2, GROUPS)), dma((2, 2, GROUPS)), dma((2, 2, GROUPS)),
+            dma((2, GROUPS)), dma((2, GROUPS)),
+        ],
+        compiler_params=pltpu.CompilerParams(
+            collective_id=0, has_side_effects=True, vmem_limit_bytes=60 * 1024 * 1024
+        ),
+        cost_estimate=pl.CostEstimate(flops=50 * 10**9, bytes_accessed=18 * 2**20, transcendentals=0),
+        name="dispatch",
+    )(main, tail, gate, up, down)
+
+
+def reply_kernel(main_ref, tail_ref, got_ref, end_ref, own_sem, put_send, put_recv):
+    e, x = lax.axis_index("ep"), lax.axis_index("tp")
+    n = main_ref.shape[0]
+    barrier = pltpu.get_barrier_semaphore()
+
+    def greet(k, _):
+        pl.semaphore_signal(barrier, inc=1, device_id=(e ^ k, x), device_id_type=MESH)
+        return 0
+
+    lax.fori_loop(1, n, greet, 0)
+    pl.semaphore_wait(barrier, n - 1)
+    pairs = ((main_ref, got_ref), (tail_ref, end_ref))
+    own = [pltpu.make_async_copy(src.at[0], dst.at[0], own_sem.at[w]) for w, (src, dst) in enumerate(pairs)]
+    for c in own:
+        c.start()
+
+    def put(k, _):
+        for w, (src, dst) in enumerate(pairs):
+            pltpu.make_async_remote_copy(
+                src_ref=src.at[k], dst_ref=dst.at[k], send_sem=put_send.at[w], recv_sem=put_recv.at[w],
+                device_id=(e ^ k, x), device_id_type=MESH,
+            ).start()
+        return 0
+
+    lax.fori_loop(1, n, put, 0)
+    for c in own:
+        c.wait()
+    for w, (src, dst) in enumerate(pairs):
+        moved = dst.at[pl.ds(1, n - 1)]
+        pltpu.make_async_copy(moved, moved, put_recv.at[w]).wait()
+        pltpu.make_async_copy(moved, moved, put_send.at[w]).wait()
+
+
+def send_back(main, tail):
+    dma = pltpu.SemaphoreType.DMA
+    return pl.pallas_call(
+        reply_kernel,
+        out_shape=(jax.ShapeDtypeStruct(main.shape, BF), jax.ShapeDtypeStruct(tail.shape, BF)),
+        in_specs=[pl.BlockSpec(memory_space=pltpu.HBM)] * 2,
+        out_specs=(pl.BlockSpec(memory_space=pltpu.VMEM),) * 2,
+        scratch_shapes=[dma((2,)), dma((2,)), dma((2,))],
+        compiler_params=pltpu.CompilerParams(
+            collective_id=1, has_side_effects=True, vmem_limit_bytes=8 * 2**20
+        ),
+        cost_estimate=pl.CostEstimate(flops=10 * 10**9, bytes_accessed=3 * 2**20, transcendentals=0),
+        name="replies",
+    )(main, tail)
 
 
 def per_device(
     queries, key_rows, value_rows, lambdas, head_gain, out_weight, moe_input, moe_gain,
     routes, route_logits, expert_gate, expert_up, expert_down,
 ):
-    model_width = out_weight.shape[1]
+    width = out_weight.shape[1]
+    token_count, top_count = routes.shape
+    n = lax.axis_size("ep")
     attended = attend(queries, key_rows, value_rows, lambdas, head_gain)
-    token_count, top_count = routes.shape
-    experts_all = lax.axis_size("ep")
-    slot_count = capacity(token_count, top_count, experts_all)
     moe_float = moe_input.astype(F32)
     normed = (
         moe_float
@@ -137,32 +339,31 @@
     ).astype(BF)
     gate_weights = jax.nn.softmax(route_logits, axis=-1)
     flat_routes = routes.reshape(-1)
-    chosen = (flat_routes[:, None] == jnp.arange(experts_all, dtype=jnp.int32)[None, :]).astype(jnp.int32)
-    slot_rank = jnp.sum((jnp.cumsum(chosen, axis=0) - chosen) * chosen, axis=1)
-    slot_ids = (flat_routes * slot_count + slot_rank).reshape(token_count, top_count)
-    dispatch = jnp.any(
-        slot_ids[None, :, :] == jnp.arange(experts_all * slot_count, dtype=jnp.int32)[:, None, None],
-        axis=-1,
+    chosen = (flat_routes[:, None] == jnp.arange(n, dtype=jnp.int32)[None, :]).astype(jnp.int32)
+    rank = jnp.sum((jnp.cumsum(chosen, axis=0) - chosen) * chosen, axis=1)
+    step = flat_routes ^ lax.axis_index("ep")
+    place = jnp.where(rank < MAIN, step * MAIN + rank, n * MAIN + step * 2 + rank - MAIN)
+    place = place.reshape(token_count, top_count)
+    slots = jnp.arange(n * (MAIN + 2), dtype=jnp.int32)
+    dispatch = jnp.any(place[None, :, :] == slots[:, None, None], axis=-1).astype(BF)
+    outgoing = jnp.dot(dispatch, normed, preferred_element_type=F32).astype(BF)
+    part = front(
+        outgoing[: n * MAIN].reshape(n, MAIN, width), outgoing[n * MAIN :].reshape(n, 2, width),
+        expert_gate[0], expert_up[0], expert_down[0],
+    )
+    reply = lax.psum_scatter(part.reshape(-1, width), "tp", scatter_dimension=0, tiled=True)
+    got, got_end = send_back(
+        reply[: n * MAIN].reshape(n, MAIN, width), reply[n * MAIN :].reshape(n, 2, width)
+    )
+    weights = jnp.sum(
+        jnp.where(place[:, :, None] == slots, gate_weights[:, :, None], 0.0), axis=1
+    )
+    high = weights.astype(BF)
+    low = (weights - high.astype(F32)).astype(BF)
+    both = jnp.concatenate([got.reshape(n * MAIN, width), got_end.reshape(n * 2, width)], axis=0)
+    expert_out = (
+        jnp.dot(high, both, preferred_element_type=F32) + jnp.dot(low, both, preferred_element_type=F32)
     ).astype(BF)
-    outgoing = jnp.dot(dispatch, normed, preferred_element_type=F32).astype(BF)
-    arrived = lax.all_to_all(outgoing, "ep", split_axis=0, concat_axis=0, tiled=True)
-    segment = lax.all_gather(arrived, "tp", axis=0, tiled=True)
-    gate_part = jnp.dot(segment, expert_gate[0], preferred_element_type=F32)
-    up_part = jnp.dot(segment, expert_up[0], preferred_element_type=F32)
-    hidden = (jax.nn.silu(gate_part) * up_part).astype(BF)
-    expert_part = jnp.dot(hidden, expert_down[0], preferred_element_type=F32).astype(BF)
-    reply = lax.psum_scatter(expert_part, "tp", scatter_dimension=0, tiled=True)
-    replies = lax.all_to_all(reply, "ep", split_axis=0, concat_axis=0, tiled=True)
-    weights = jnp.sum(
-        jnp.where(
-            slot_ids[:, :, None] == jnp.arange(experts_all * slot_count, dtype=jnp.int32),
-            gate_weights[:, :, None],
-            0.0,
-        ),
-        axis=1,
-    )
-    picked = jnp.take(replies, slot_ids.reshape(-1), axis=0).reshape(token_count, top_count, model_width)
-    expert_out = jnp.sum(gate_weights[:, :, None] * picked.astype(F32), axis=1).astype(BF)
     mixer_part = lax.dot_general(
         attended, out_weight, (((0,), (0,)), ((), ())), preferred_element_type=F32
     ).astype(BF)

time: 319 us -> 213 us (0.67)
  waiting for transfers between devices: 128 us -> 14.5 us
  Pallas kernels: 67.7 us -> 161 us
  blocking collectives: 37.9 us -> 0 us
  matrix products: 32.7 us -> 4.43 us
  local copies, waits for them, and re-layouts: 20.7 us -> 12.1 us
  starting transfers between devices: 7.92 us -> 1.23 us
  other arithmetic: 9.26 us -> 3.59 us
    pallas_call x0 -> x2, Pallas kernels: none -> 93.6 us  [the longest x1 67.1 us: front(): pl.pallas_call(front_kernel, out_shape=jax.ShapeDtypeStruct((4, n * (MAIN...]
    all_gather x1 -> x0, waiting for transfers between devices: 53.1 us -> none  [per_device(): segment = lax.all_gather(arrived, 'tp', axis=0, tiled=True)]
    all_to_all x1 -> x0, blocking collectives: 37.9 us -> none  [per_device(): lax.all_to_all(outgoing, 'ep', split_axis=0, concat_axis=0, tiled=True)]
    all_gather x1, waiting for transfers between devices: 42.9 us -> 10.7 us  [attend(): lax.all_gather(packed, 'ep', axis_index_groups=groups, axis=0, tiled=True)]
    all_to_all x1 -> x0, waiting for transfers between devices: 28.1 us -> none  [per_device(): lax.all_to_all(reply, 'ep', split_axis=0, concat_axis=0, tiled=True)]
    dot_general x2, matrix products: 27.9 us -> 1.75 us  [the longest x1 1.28 us: per_device(): jnp.dot(low, both, preferred_element_type=F32)]
    all_to_all x4 -> x0, local copies, waits for them, and re-layouts: 11.8 us -> none  [the longest x2 5.93 us: per_device(): lax.all_to_all(outgoing, 'ep', split_axis=0, concat_axis=0, tiled=True)]
    all_to_all x1 -> x0, starting transfers between devices: 5.76 us -> none  [per_device(): lax.all_to_all(reply, 'ep', split_axis=0, concat_axis=0, tiled=True)]
  transfers between devices with their start and end apart: 8 -> 6, of which waited for: 5 -> 3; matrix products, arithmetic and copies ran while one was open for 12% -> 6% of each run, Pallas kernels for 21% -> 76%
where the time goes in v2:
time: 213 us
  Pallas kernels  161 us (76%)
  between operations  15.8 us (7%)
  waiting for transfers between devices  14.5 us (7%)
  local copies, waits for them, and re-layouts  12.1 us (6%)
  matrix products  4.43 us (2%)
  other arithmetic  3.59 us (2%)
    pallas_call x1, Pallas kernels, attention(): pl.pallas_call(functools.partial(attn_kernel, nq=nq, nblk=nblk, kb=kb, qt...  67.7 us
    pallas_call x1, Pallas kernels, front(): pl.pallas_call(front_kernel, out_shape=jax.ShapeDtypeStruct((4, n * (MAIN...  67.1 us
    pallas_call x1, Pallas kernels, send_back(): pl.pallas_call(reply_kernel, out_shape=(jax.ShapeDtypeStruct(main.shape,...  26.5 us
    all_gather x1, waiting for transfers between devices, attend(): lax.all_gather(packed, 'ep', axis_index_groups=groups, axis=0, tiled=True)  10.7 us
    unnamed x21, local copies, waits for them, and re-layouts  5.5 us
  transfers between devices with their start and end apart: 6, of which 3 were waited for; matrix products, arithmetic and copies ran while one was open for 6% of the time, Pallas kernels for 76%

profile of v2, /device:TPU:1, one launch (start us, length us, event | category | flops | bytes accessed | tf_op | source)
XLA Modules:
  0.0 212.8 jit_solution(14252727780735651732)
XLA Ops:
  8.0 0.0 all-gather.2.cloned.1.call-start
  8.1 1.1 fusion.24
  9.2 0.1 copy.40
  9.3 0.1 copy.39
  9.4 1.8 pad_maximum_fusion.4
  11.2 0.0 reduce-scatter.5.cloned.1.call-start
  11.3 0.1 copy.41
  11.4 0.1 eq.51
  11.5 0.1 eq.55
  11.7 0.6 reduce-window.6
  12.3 0.2 slice_reduce_fusion
  12.5 0.1 fusion.13
  12.6 0.1 reduce_sum.49
  12.7 0.1 copy.44
  12.8 0.1 fusion.8
  12.9 0.2 fusion.1
  13.1 0.6 convolution_convert_fusion.1
  13.7 0.9 reshape.108.tail_ref
  14.6 1.0 slice_bitcast_fusion.1.main_ref
  15.6 67.1 %dispatch.1 = bf16[4,320,2048]{2,1,0:T(8,128)(2,1)} custom-call(bf16[32,8,2048]{2,1,0:T(8,128)(2,1)} %slice_bitcast_fusion.1.main_ref, bf16[32,2,2048]{2,1,0:T(2,128)(2,1)} %reshape.108.tail_ref, bf16[2048,896]{1,0:T(8,128)(2,1)} %bitcast.47, bf16[2048,896]{1,0:T(8,128)(2,1)} %bitcast.48, bf16[896,2048]{1,0:T(8,128)(2,1)} %bitcast.49), custom_call_target="tpu_custom_call" | custom-call | flops 49999998976 | bytes 18874368 | tf_op jit(solution)/shard_map/dispatch/pallas_call | solution.py:258
  82.7 0.0 reduce-scatter.5.cloned.1.call-update
  82.8 0.0 reduce-scatter.3.cloned.1.call-start
  82.8 0.9 copy-done.3
  83.7 0.1 copy.38
  83.9 0.1 collective-permute-start
  84.0 1.5 collective-permute-done
  85.5 0.1 pad_maximum_fusion.3.q_ref
  85.6 10.7 %all-gather.2.cloned.1.call-done = bf16[16384,256]{1,0:T(8,128)(2,1)} async-done(((bf16[1024,256]{1,0:T(8,128)(2,1)}), bf16[16384,256]{1,0:T(8,128)(2,1)}) %all-gather.2.cloned.1.call-update) | async-done | bytes 8388624 | tf_op jit(solution)/shard_map/all_gather | solution.py:99
  96.3 3.5 %copy-done.1 = bf16[16384,256]{1,0:T(8,128)(2,1)S(1)} copy-done((bf16[16384,256]{1,0:T(8,128)(2,1)S(1)}, bf16[16384,256]{1,0:T(8,128)(2,1)}, u32[]{:S(2)}) %copy-start.1) | copy-done | bytes 8388632
  99.8 67.7 %attention.1 = (f32[4,128,1024]{2,1,0:T(8,128)S(1)}, f32[8,8,1024]{2,1,0:T(8,128)S(1)}) custom-call(bf16[256,1024]{1,0:T(8,128)(2,1)S(1)} %pad_maximum_fusion.3.q_ref, bf16[16,1024,256]{2,1,0:T(8,128)(2,1)S(1)} %bitcast.41), custom_call_target="tpu_custom_call" | custom-call | flops 12884901888 | bytes 16777216 | tf_op jit(solution)/shard_map/attention/pallas_call | solution.py:81
  167.4 0.1 slice.61
  167.6 0.9 collective-permute-start.2
  168.5 0.1 collective-permute-start.1
  168.6 2.2 %collective-permute-done.1 = f32[8,512]{1,0:T(8,128)S(1)} collective-permute-done((f32[8,512]{1,0:T(8,128)S(1)}, f32[8,512]{1,0:T(8,128)S(1)}, u32[]{:S(2)}, u32[]{:S(2)}) %collective-permute-start.1) | collective-permute-done | bytes 16416 | tf_op jit(solution)/shard_map/ppermute | solution.py:107
  170.8 0.3 add_divide_fusion
  171.1 0.2 multiply_reduce_fusion
  171.3 0.2 copy-done.8
  171.5 0.2 multiply_convert_fusion
  171.7 2.1 convolution_convert_fusion
  173.8 0.7 copy-done.4
  174.5 0.0 reduce-scatter.5.cloned.1.call-done
  174.6 1.0 slice.83
  175.6 0.2 reshape.111.tail_ref
  175.7 1.3 slice_bitcast_fusion.main_ref
  177.0 26.5 %replies.1 = (bf16[32,8,2048]{2,1,0:T(8,128)(2,1)S(1)}, bf16[32,2,2048]{2,1,0:T(2,128)(2,1)S(1)}) custom-call(bf16[32,8,2048]{2,1,0:T(8,128)(2,1)S(1)} %slice_bitcast_fusion.main_ref, bf16[32,2,2048]{2,1,0:T(2,128)(2,1)S(1)} %reshape.111.tail_ref), custom_call_target="tpu_custom_call" | custom-call | flops 10000000000 | bytes 3145728 | tf_op jit(solution)/shard_map/replies/pallas_call | solution.py:312
  203.5 0.1 reshape.113
  203.6 0.5 fusion.4
  204.1 1.3 fusion
  (34 shorter events, 0.3 us)
Async XLA Ops:
  8.0 163.7 %copy-start = (bf16[256,2048]{1,0:T(8,128)(2,1)S(1)}, bf16[256,2048]{1,0:T(8,128)(2,1)}, u32[]{:S(2)}) copy-start(bf16[256,2048]{1,0:T(8,128)(2,1)} %param.18) | copy-start | bytes 3145732
  8.0 3.2 %copy-start.6 = (s32[128,2]{0,1:T(2,128)S(1)}, s32[128,2]{0,1:T(2,128)}, u32[]{:S(2)}) copy-start(s32[128,2]{0,1:T(2,128)} %param.21) | copy-start | bytes 3076
  8.0 4.9 %copy-start.2 = (bf16[128,2048]{1,0:T(8,128)(2,1)S(1)}, bf16[128,2048]{1,0:T(8,128)(2,1)}, u32[]{:S(2)}) copy-start(bf16[128,2048]{1,0:T(8,128)(2,1)} %param.19) | copy-start | bytes 1572868
  8.0 5.1 %copy-start.5 = (f32[2048]{0:T(1024)S(1)}, f32[2048]{0:T(1024)}, u32[]{:S(2)}) copy-start(f32[2048]{0:T(1024)} %param.20) | copy-start | bytes 24580
  8.0 88.2 %all-gather.2.cloned.1.call-start = ((), (), s32[]{:S(2)}) async-start(), calls=%async_computation.2 | async-start | bytes 8912896 | tf_op jit(solution)/shard_map/all_gather | solution.py:99
  11.2 163.4 %reduce-scatter.5.cloned.1.call-start = ((), (), s32[]{:S(2)}) async-start(), calls=%async_computation.4 | async-start | bytes 6553600 | tf_op jit(solution)/shard_map/reduce_scatter | solution.py:354
  82.7 1.0 copy-start.3
  82.8 122.6 %reduce-scatter.3.cloned.1.call-start = ((), (), s32[]{:S(2)}) async-start(), calls=%async_computation.3 | async-start | bytes 2621440 | tf_op jit(solution)/shard_map/reduce_scatter | solution.py:370
  83.9 1.6 collective-permute-start
  96.3 3.5 %copy-start.1 = (bf16[16384,256]{1,0:T(8,128)(2,1)S(1)}, bf16[16384,256]{1,0:T(8,128)(2,1)}, u32[]{:S(2)}) copy-start(bf16[16384,256]{1,0:T(8,128)(2,1)} %all-gather.2.cloned.1.call-done) | copy-start | bytes 25165828
  167.5 3.6 %copy-start.7 = (f32[2]{0:T(128)S(1)}, f32[2]{0:T(128)}, u32[]{:S(2)}) copy-start(f32[2]{0:T(128)} %param.16) | copy-start | bytes 28
  167.6 3.3 %collective-permute-start.2 = (f32[4,128,512]{2,1,0:T(8,128)S(1)}, f32[4,128,512]{2,1,0:T(8,128)S(1)}, u32[]{:S(2)}, u32[]{:S(2)}) collective-permute-start(f32[4,128,512]{2,1,0:T(8,128)S(1)} %slice.61), channel_id=1, source_target_pairs={{0,4},{4,0},{8,12},{12,8},{16,20},{20,16},{24,28},{28,24},{32,36},... | collective-permute-start | bytes 3145736 | tf_op jit(solution)/shard_map/ppermute | solution.py:106
  168.5 2.3 %collective-permute-start.1 = (f32[8,512]{1,0:T(8,128)S(1)}, f32[8,512]{1,0:T(8,128)S(1)}, u32[]{:S(2)}, u32[]{:S(2)}) collective-permute-start(f32[8,512]{1,0:T(8,128)S(1)} %slice.75), channel_id=1, source_target_pairs={{0,4},{4,0},{8,12},{12,8},{16,20},{20,16},{24,28},{28,24},{32,36},... | collective-permute-start | bytes 49160 | tf_op jit(solution)/shard_map/ppermute | solution.py:107
  170.8 0.7 copy-start.8
  173.8 0.7 copy-start.4
Sparse Core Ops, SparseCore 0:
  11.6 84.6 all-gather.1
Sparse Core Ops, SparseCore 1:
  82.8 53.6 reduce-scatter.4
  173.9 28.7 reduce-scatter.2

commit v3 on v2

--- a/solution.py
+++ b/solution.py
@@ -12,15 +12,21 @@
 init_lambda = 0.2
 LIM = 100.0
 LOG2E = 1.4426950408889634
-def attn_kernel(q_ref, kv_ref, o_ref, st_ref, acc_ref, *, nq, nblk, kb, qt):
+def attn_kernel(mine_ref, far_ref, k_ref, v_ref, o_ref, st_ref, acc_ref, *, nq, nblk, kb, qt):
+    def both(rows):
+        return jnp.concatenate([mine_ref[rows], far_ref[rows]], axis=1)
+
+    def other(b):
+        return (b % 4) * 4 + b // 4
+
     lane_id = lax.broadcasted_iota(jnp.int32, (256, 128), 0) // 64
     pick = (lane_id == lax.broadcasted_iota(jnp.int32, (256, 128), 1)).astype(BF)
     def norms(b, best):
-        k = kv_ref[b, :kb, :].astype(F32)
+        k = k_ref[b].astype(F32)
         kk = jnp.dot((k * k).astype(BF), pick, preferred_element_type=F32)
         return jnp.maximum(best, jnp.max(kk, axis=0, keepdims=True))
     kmax = lax.fori_loop(0, nblk, norms, jnp.zeros((1, 128), F32))
-    qf = q_ref[...].astype(F32)
+    qf = both(slice(0, 256)).astype(F32)
     qq = jnp.sum((qf * qf).reshape(4, 64, nq), axis=1)
     bound2 = jnp.max(qq) * jnp.max(kmax) * (LOG2E * LOG2E * 1.05)
     small = bound2 < LIM * LIM
@@ -28,7 +34,7 @@
     ones = jnp.ones((16, 256), BF)
 
     def head_queries(h, i):
-        qh = q_ref[128 * h:128 * h + 128, :]
+        qh = both(slice(128 * h, 128 * h + 128))
         return jnp.where((row // 64) == i, qh, jnp.zeros_like(qh))
 
     @pl.when(small)
@@ -37,8 +43,8 @@
             qs = [head_queries(h, i) for i in range(2)]
             acc_ref[...] = jnp.zeros_like(acc_ref)
             def body(b, _):
-                kh = kv_ref[b, :kb, 128 * h:128 * h + 128]
-                vts = [jnp.concatenate([kv_ref[b, kb + 256 * t + 128 * h: kb + 256 * t + 128 * h + 128, :], ones], 0) for t in range(kb // 256)]
+                kh = k_ref[b, :, 128 * h:128 * h + 128]
+                vts = [jnp.concatenate([v_ref[other(b), 256 * t + 128 * h: 256 * t + 128 * h + 128, :], ones], 0) for t in range(kb // 256)]
                 for i in range(2):
                     for j in range(nq // qt):
                         s = jnp.dot(kh, qs[i][:, j * qt:(j + 1) * qt], preferred_element_type=F32)
@@ -60,13 +66,13 @@
                 for j in range(nq // qt):
                     acc_ref[i, :, j * qt:(j + 1) * qt] = jnp.zeros((144, qt), F32)
                     def body(b, m):
-                        kh = kv_ref[b, :kb, 128 * h:128 * h + 128]
+                        kh = k_ref[b, :, 128 * h:128 * h + 128]
                         s = jnp.dot(kh, qi[:, j * qt:(j + 1) * qt], preferred_element_type=F32)
                         mn = jnp.maximum(m, jnp.max(s, axis=0, keepdims=True))
                         p = jnp.exp2((s - mn) * LOG2E).astype(BF)
                         add = 0.0
                         for t in range(kb // 256):
-                            vt = jnp.concatenate([kv_ref[b, kb + 256 * t + 128 * h: kb + 256 * t + 128 * h + 128, :], ones], 0)
+                            vt = jnp.concatenate([v_ref[other(b), 256 * t + 128 * h: 256 * t + 128 * h + 128, :], ones], 0)
                             add = add + jnp.dot(vt, p[256 * t:256 * t + 256], preferred_element_type=F32)
                         acc_ref[i, :, j * qt:(j + 1) * qt] = acc_ref[i, :, j * qt:(j + 1) * qt] * jnp.exp2((m - mn) * LOG2E) + add
                         return mn
@@ -76,32 +82,26 @@
                     st_ref[2 * h + i, :, sl] = acc_ref[i, 128:136, sl]
                     st_ref[4 + 2 * h + i, :, sl] = jnp.broadcast_to(m, (8, qt))
 
-def attention(qT, kv, qt=1024):
-    nq = qT.shape[1]; nblk, kb2, _ = kv.shape; kb = kb2 // 2
+def attention(mine, far, keys, values, qt=1024):
+    nq = 2 * mine.shape[1]
+    nblk, kb, _ = keys.shape
     return pl.pallas_call(
         functools.partial(attn_kernel, nq=nq, nblk=nblk, kb=kb, qt=qt),
         out_shape=(jax.ShapeDtypeStruct((4, 128, nq), F32), jax.ShapeDtypeStruct((8, 8, nq), F32)),
-        in_specs=[pl.BlockSpec(memory_space=pltpu.VMEM)] * 2,
+        in_specs=[pl.BlockSpec(memory_space=pltpu.VMEM)] * 4,
         out_specs=(pl.BlockSpec(memory_space=pltpu.VMEM),) * 2,
         scratch_shapes=[pltpu.VMEM((2, 144, nq), F32)],
         compiler_params=pltpu.CompilerParams(vmem_limit_bytes=40 * 2**20),
         cost_estimate=pl.CostEstimate(flops=4 * nblk * kb * nq * 4 * 192 // 2, bytes_accessed=16 * 2**20, transcendentals=4 * nblk * kb * nq),
         name="attention",
-    )(qT, kv)
-
-
-def attend(queries, key_rows, value_rows, lambdas, head_gain):
-    rows = queries.shape[0]
+    )(mine, far, keys, values)
+
+
+def attend(mine, far, keys, values, lambdas, head_gain):
+    rows = mine.shape[1]
     n = lax.axis_size("ep")
-    keys_t = value_rows.T
-    packed = jnp.concatenate([key_rows, keys_t[:, :256], keys_t[:, 256:]], axis=0)
-    groups = [[2 * k + c for k in range(n // 2)] for c in range(2)]
-    kv = lax.all_gather(packed, "ep", axis_index_groups=groups, axis=0, tiled=True)
-    kv = kv.reshape(n // 2, 2 * rows, 256)
     swap = [(k, k ^ 1) for k in range(n)]
-    mine = (queries * jnp.asarray(0.125, BF)).T
-    other = lax.ppermute(mine, "ep", swap)
-    out, stats = attention(jnp.concatenate([mine, other], axis=1), kv)
+    out, stats = attention(mine, far, keys, values)
     stats = stats[:, 0]
     far_out = lax.ppermute(out[:, :, rows:], "ep", swap)
     far_stats = lax.ppermute(stats[:, rows:], "ep", swap)
@@ -122,8 +122,10 @@
 
 
 def front_kernel(
-    main_ref, tail_ref, gate_ref, up_ref, down_ref, out_ref, seg_ref, end_ref, g_buf, u_buf, d_buf,
+    main_ref, tail_ref, gate_ref, up_ref, down_ref, key_ref, value_ref, mine_ref,
+    out_ref, keys_ref, values_ref, far_ref, seg_ref, end_ref, g_buf, u_buf, d_buf,
     own_sem, load_sem, put_send, put_recv, near_send, near_recv, far_send, far_recv,
+    home_sem, swap_sem, one_send, one_recv, onef_send, onef_recv, two_send, two_recv, twof_send, twof_recv,
 ):
     e, x = lax.axis_index("ep"), lax.axis_index("tp")
     n = main_ref.shape[0]
@@ -132,6 +134,120 @@
     right, left = lax.rem(x + 1, 4), lax.rem(x + 3, 4)
     across = lax.rem(x + 2, 4)
     barrier = pltpu.get_barrier_semaphore()
+
+    core, y, z = lax.rem(e, 2), lax.rem(e // 2, 4), e // 8
+
+    def chip(dz, dy):
+        return (lax.rem(z + dz, 4) * 4 + lax.rem(y + dy, 4)) * 2 + core, x
+
+    half = key_ref.shape[0] // 2
+    home = [
+        pltpu.make_async_copy(key_ref, keys_ref.at[z, y], home_sem.at[0]),
+        pltpu.make_async_copy(value_ref, values_ref.at[y, z], home_sem.at[1]),
+    ]
+    swap = pltpu.make_async_remote_copy(
+        src_ref=mine_ref, dst_ref=far_ref, send_sem=swap_sem.at[0], recv_sem=swap_sem.at[1],
+        device_id=(e ^ 1, x), device_id_type=MESH,
+    )
+    ends = (keys_ref, values_ref)
+    firsts = (key_ref, value_ref)
+    inner, outer = (y, z), (z, y)
+
+    def along(w, step, second):
+        return chip(step, 0) if (w == 0) == second else chip(0, step)
+
+    def hop(src, dst, sems, w, step, second):
+        return pltpu.make_async_remote_copy(
+            src_ref=src, dst_ref=dst, send_sem=sems[0], recv_sem=sems[1],
+            device_id=along(w, step, second), device_id_type=MESH,
+        )
+
+    def rows_of(g):
+        return pl.ds(g * half, half)
+
+    def arrival(dst, sem):
+        return pltpu.make_async_copy(dst, dst, sem)
+
+    def one_near(w, g, d):
+        dst = ends[w].at[outer[w], inner[w], rows_of(g)]
+        return hop(firsts[w].at[rows_of(g)], dst, (one_send.at[w, d, g], one_recv.at[w, d, g]), w, 1 if d == 0 else 3, False)
+
+    def one_slot(w, g, step):
+        return ends[w].at[outer[w], lax.rem(inner[w] + step, 4), rows_of(g)]
+
+    def one_came(w, g, d):
+        return arrival(one_slot(w, g, 3 if d == 0 else 1), one_recv.at[w, d, g])
+
+    def one_far(w, g):
+        part = one_slot(w, g, 3 if g == 0 else 1)
+        return hop(part, part, (onef_send.at[w, g], onef_recv.at[w, g]), w, 1 if g == 0 else 3, False)
+
+    def two_slot(w, r, step):
+        return ends[w].at[lax.rem(outer[w] + step, 4), lax.rem(inner[w] + r, 4)]
+
+    def two_near(w, r, d):
+        src = firsts[w] if r == 0 else two_slot(w, r, 0)
+        return hop(src, two_slot(w, r, 0), (two_send.at[w, d, r], two_recv.at[w, d, r]), w, 1 if d == 0 else 3, True)
+
+    def two_came(w, r, d):
+        return arrival(two_slot(w, r, 3 if d == 0 else 1), two_recv.at[w, d, r])
+
+    def via(r):
+        return 0 if r in (0, 1) else 1
+
+    def two_far(w, r):
+        d = via(r)
+        part = two_slot(w, r, 3 if d == 0 else 1)
+        return hop(part, part, (twof_send.at[w, r], twof_recv.at[w, r]), w, 1 if d == 0 else 3, True)
+
+    def spread_first():
+        for c in home:
+            c.start()
+        for w in range(2):
+            for g in range(2):
+                for d in range(2):
+                    one_near(w, g, d).start()
+        for w in range(2):
+            for d in range(2):
+                two_near(w, 0, d).start()
+
+    def spread_near():
+        for w in range(2):
+            for g in range(2):
+                one_came(w, g, g).wait()
+                one_far(w, g).start()
+        for r in (1, 3):
+            for w in range(2):
+                one_came(w, 1 - (0 if r == 3 else 1), 0 if r == 3 else 1).wait()
+                for d in range(2):
+                    two_near(w, r, d).start()
+
+    def spread_across():
+        for w in range(2):
+            for g in range(2):
+                arrival(one_slot(w, g, 2), onef_recv.at[w, g]).wait()
+            for d in range(2):
+                two_near(w, 2, d).start()
+
+    def spread_relay(r):
+        for w in range(2):
+            two_came(w, r, via(r)).wait()
+            two_far(w, r).start()
+
+    def spread_end():
+        for w in range(2):
+            home[w].wait()
+            for r in range(4):
+                two_came(w, r, 1 - via(r)).wait()
+                arrival(two_slot(w, r, 2), twof_recv.at[w, r]).wait()
+                two_far(w, r).wait_send()
+                for d in range(2):
+                    two_near(w, r, d).wait_send()
+            for g in range(2):
+                one_far(w, g).wait_send()
+                for d in range(2):
+                    one_near(w, g, d).wait_send()
+        swap.wait()
 
     def greet(k, _):
         pl.semaphore_signal(barrier, inc=1, device_id=(e ^ k, x), device_id_type=MESH)
@@ -156,6 +272,8 @@
             return 0
 
         lax.fori_loop(max(1, g * per), g * per + per, put, 0)
+    swap.start()
+    spread_first()
     loads = [
         pltpu.make_async_copy(src, dst, load_sem.at[k])
         for k, (src, dst) in enumerate(((gate_ref, g_buf), (up_ref, u_buf), (down_ref, d_buf)))
@@ -210,18 +328,24 @@
         def _():
             for g in range(GROUPS - 3, GROUPS):
                 relay(g)
+            spread_near()
+            spread_relay(0)
             for w in range(2):
                 for g in range(0, GROUPS, 2):
                     came(w, g, 1).wait()
 
         @pl.when(t == 2)
         def _():
+            spread_across()
+            spread_relay(1)
             for w in range(2):
                 for g in range(1, GROUPS, 2):
                     came(w, g, 0).wait()
 
         @pl.when(t == 3)
         def _():
+            spread_relay(3)
+            spread_relay(2)
             for w in range(2):
                 for g in range(GROUPS):
                     part = pairs[w][1].at[across, span(g)]
@@ -238,6 +362,7 @@
         return 0
 
     lax.fori_loop(0, 4, expert, 0)
+    spread_end()
     for w, (src, dst) in enumerate(pairs):
         sent = dst.at[x, pl.ds(1, n - 1)]
         pltpu.make_async_copy(sent, sent, put_send.at[w]).wait()
@@ -251,27 +376,34 @@
     return t + (t // 2) * (1 - 2 * (t % 2))
 
 
-def front(main, tail, gate, up, down):
+def front(main, tail, gate, up, down, key, value, mine):
     n, _, width = main.shape
     dma = pltpu.SemaphoreType.DMA
     hbm = pl.BlockSpec(memory_space=pl.ANY)
     return pl.pallas_call(
         front_kernel,
-        out_shape=jax.ShapeDtypeStruct((4, n * (MAIN + 2), width), BF),
-        in_specs=[hbm] * 5,
-        out_specs=pl.BlockSpec(memory_space=pltpu.VMEM),
+        out_shape=(
+            jax.ShapeDtypeStruct((4, n * (MAIN + 2), width), BF),
+            jax.ShapeDtypeStruct((4, 4, *key.shape), BF),
+            jax.ShapeDtypeStruct((4, 4, *value.shape), BF),
+            jax.ShapeDtypeStruct(mine.shape, BF),
+        ),
+        in_specs=[hbm] * 8,
+        out_specs=(pl.BlockSpec(memory_space=pltpu.VMEM), hbm, hbm, hbm),
         scratch_shapes=[
             pltpu.VMEM((4, n, MAIN, width), BF), pltpu.VMEM((4, n, 2, width), BF),
             pltpu.VMEM(gate.shape, BF), pltpu.VMEM(up.shape, BF), pltpu.VMEM(down.shape, BF),
             dma((2,)), dma((3,)), dma((2,)), dma((2, GROUPS)), dma((2, 2, GROUPS)), dma((2, 2, GROUPS)),
             dma((2, GROUPS)), dma((2, GROUPS)),
+            dma((2,)), dma((2,)), dma((2, 2, 2)), dma((2, 2, 2)), dma((2, 2)), dma((2, 2)),
+            dma((2, 2, 4)), dma((2, 2, 4)), dma((2, 4)), dma((2, 4)),
         ],
         compiler_params=pltpu.CompilerParams(
             collective_id=0, has_side_effects=True, vmem_limit_bytes=60 * 1024 * 1024
         ),
         cost_estimate=pl.CostEstimate(flops=50 * 10**9, bytes_accessed=18 * 2**20, transcendentals=0),
         name="dispatch",
-    )(main, tail, gate, up, down)
+    )(main, tail, gate, up, down, key, value, mine)
 
 
 def reply_kernel(main_ref, tail_ref, got_ref, end_ref, own_sem, put_send, put_recv):
@@ -330,7 +462,6 @@
     width = out_weight.shape[1]
     token_count, top_count = routes.shape
     n = lax.axis_size("ep")
-    attended = attend(queries, key_rows, value_rows, lambdas, head_gain)
     moe_float = moe_input.astype(F32)
     normed = (
         moe_float
@@ -347,9 +478,15 @@
     slots = jnp.arange(n * (MAIN + 2), dtype=jnp.int32)
     dispatch = jnp.any(place[None, :, :] == slots[:, None, None], axis=-1).astype(BF)
     outgoing = jnp.dot(dispatch, normed, preferred_element_type=F32).astype(BF)
-    part = front(
+    mine = (queries * jnp.asarray(0.125, BF)).T
+    values_t = value_rows.T
+    value = jnp.concatenate([values_t[:, :256], values_t[:, 256:]], axis=0)
+    part, keys, values, far = front(
         outgoing[: n * MAIN].reshape(n, MAIN, width), outgoing[n * MAIN :].reshape(n, 2, width),
-        expert_gate[0], expert_up[0], expert_down[0],
+        expert_gate[0], expert_up[0], expert_down[0], key_rows, value, mine,
+    )
+    attended = attend(
+        mine, far, keys.reshape(16, 512, 256), values.reshape(16, 512, 256), lambdas, head_gain
     )
     reply = lax.psum_scatter(part.reshape(-1, width), "tp", scatter_dimension=0, tiled=True)
     got, got_end = send_back(

time: 213 us -> 223 us (1.047)
  Pallas kernels: 161 us -> 182 us
  waiting for transfers between devices: 14.5 us -> 2.22 us
    pallas_call x1, Pallas kernels: 67.1 us -> 90.2 us  [front(): pl.pallas_call(front_kernel, out_shape=(jax.ShapeDtypeStruct((4, n * (MAI...]
    all_gather x1 -> x0, waiting for transfers between devices: 10.7 us -> none  [attend(): lax.all_gather(packed, 'ep', axis_index_groups=groups, axis=0, tiled=True)]
    unnamed x21 -> x24, local copies, waits for them, and re-layouts: 5.5 us -> 7.33 us
  transfers between devices with their start and end apart: 6 -> 4, of which waited for: 3 -> 1; matrix products, arithmetic and copies ran while one was open for 6% -> 3% of each run, Pallas kernels for 76% -> 41%
where the time goes in v3:
time: 223 us
  Pallas kernels  182 us (82%)
  between operations  14.3 us (6%)
  local copies, waits for them, and re-layouts  12.6 us (6%)
  matrix products  5.53 us (2%)
  other arithmetic  4.9 us (2%)
    pallas_call x1, Pallas kernels, front(): pl.pallas_call(front_kernel, out_shape=(jax.ShapeDtypeStruct((4, n * (MAI...  90.2 us
    pallas_call x1, Pallas kernels, attention(): pl.pallas_call(functools.partial(attn_kernel, nq=nq, nblk=nblk, kb=kb, qt...  67 us
    pallas_call x1, Pallas kernels, send_back(): pl.pallas_call(reply_kernel, out_shape=(jax.ShapeDtypeStruct(main.shape,...  24.9 us
    unnamed x24, local copies, waits for them, and re-layouts  7.33 us
  transfers between devices with their start and end apart: 4, of which 1 were waited for; matrix products, arithmetic and copies ran while one was open for 3% of the time, Pallas kernels for 41%

profile of v3, /device:TPU:1, one launch (start us, length us, event | category | flops | bytes accessed | tf_op | source)
XLA Modules:
  0.0 222.5 jit_solution(5441809012422202189)
XLA Ops:
  7.2 0.0 copy-start
  7.2 0.0 reduce-scatter.5.cloned.1.call-start
  7.2 0.9 copy.36
  8.1 0.1 eq.55
  8.2 0.1 eq.51
  8.4 0.6 reduce-window.6
  9.0 0.2 slice_reduce_fusion
  9.2 0.1 fusion.13
  9.3 0.1 reduce_sum.48
  9.5 0.1 copy.39
  9.5 0.7 compare_select_fusion
  10.3 1.2 fusion.1
  11.5 1.7 convolution_convert_fusion.1
  13.2 0.0 copy-start.6
  13.2 1.0 slice_bitcast_fusion.1.main_ref
  14.3 0.9 reshape.109.tail_ref
  15.2 0.1 copy.42
  15.3 0.1 copy.35
  15.5 0.7 multiply_bitcast_fusion.mine_ref
  16.2 0.7 pad_maximum_fusion.3.value_ref
  16.9 90.2 %dispatch.1 = (bf16[4,320,2048]{2,1,0:T(8,128)(2,1)}, bf16[4,4,512,256]{3,2,1,0:T(8,128)(2,1)}, bf16[4,4,512,256]{3,2,1,0:T(8,128)(2,1)}, bf16[256,512]{1,0:T(8,128)(2,1)}) custom-call(bf16[32,8,2048]{2,1,0:T(8,128)(2,1)} %slice_bitcast_fusion.1.main_ref, bf16[32,2,2048]{2,1,0:T(2,128)(2,1)} %reshape.109.tail_ref, bf16[2048,896]{1,0:T(8,128)(2,1)} %bitcast.49, ...), custom_call_target="tpu_custom_call" | custom-call | flops 49999998976 | bytes 18874368 | tf_op jit(solution)/shard_map/dispatch/pallas_call | solution.py:383
  107.2 0.0 copy-start.1
  107.2 0.0 reduce-scatter.5.cloned.1.call-update
  107.2 0.0 reduce-scatter.3.cloned.1.call-start
  107.3 0.9 copy-done.1
  108.1 0.1 copy-done.4
  108.2 2.2 copy-done.2
  110.4 2.2 copy-done.3
  112.6 67.0 %attention.1 = (f32[4,128,1024]{2,1,0:T(8,128)S(1)}, f32[8,8,1024]{2,1,0:T(8,128)S(1)}) custom-call(bf16[256,512]{1,0:T(8,128)(2,1)S(1)} %copy-done.1, bf16[256,512]{1,0:T(8,128)(2,1)S(1)} %copy-done.4, bf16[16,512,256]{2,1,0:T(8,128)(2,1)S(1)} %bitcast.42, bf16[16,512,256]{2,1,0:T(8,128)(2,1)S(1)} %bitcast.43), custom_call_target="tpu_custom_call" | custom-call | flops 12884901888 | bytes 16777216 | tf_op jit(solution)/shard_map/attention/pallas_call | solution.py:88
  179.6 0.1 slice.65
  179.7 0.7 collective-permute-start.1
  180.4 0.1 collective-permute-start
  180.5 2.2 collective-permute-done
  182.7 0.3 add_divide_fusion
  183.0 0.2 multiply_reduce_fusion
  183.2 0.2 copy-done.9
  183.4 0.2 multiply_convert_fusion
  183.6 2.1 convolution_convert_fusion
  185.7 0.0 reduce-scatter.3.cloned.1.call-update
  185.7 0.7 copy-done.7
  186.4 0.0 reduce-scatter.5.cloned.1.call-done
  186.5 1.0 slice.83
  187.4 0.2 reshape.115.tail_ref
  187.6 1.3 slice_bitcast_fusion.main_ref
  188.9 24.9 %replies.1 = (bf16[32,8,2048]{2,1,0:T(8,128)(2,1)S(1)}, bf16[32,2,2048]{2,1,0:T(2,128)(2,1)S(1)}) custom-call(bf16[32,8,2048]{2,1,0:T(8,128)(2,1)S(1)} %slice_bitcast_fusion.main_ref, bf16[32,2,2048]{2,1,0:T(2,128)(2,1)S(1)} %reshape.115.tail_ref), custom_call_target="tpu_custom_call" | custom-call | flops 10000000000 | bytes 3145728 | tf_op jit(solution)/shard_map/replies/pallas_call | solution.py:444
  213.8 0.1 reshape.117
  213.9 0.5 fusion.4
  214.4 1.3 fusion
  (29 shorter events, 0.3 us)
Async XLA Ops:
  7.2 176.4 %copy-start = (bf16[256,2048]{1,0:T(8,128)(2,1)S(1)}, bf16[256,2048]{1,0:T(8,128)(2,1)}, u32[]{:S(2)}) copy-start(bf16[256,2048]{1,0:T(8,128)(2,1)} %param.18) | copy-start | bytes 3145732
  7.2 179.3 %reduce-scatter.5.cloned.1.call-start = ((), (), s32[]{:S(2)}) async-start(), calls=%async_computation.3 | async-start | bytes 6553600 | tf_op jit(solution)/shard_map/reduce_scatter | solution.py:491
  11.5 3.6 %copy-start.5 = (bf16[512,256]{1,0:T(8,128)(2,1)S(1)}, bf16[512,256]{1,0:T(8,128)(2,1)}, u32[]{:S(2)}) copy-start(bf16[512,256]{1,0:T(8,128)(2,1)} %param.15) | copy-start | bytes 786436
  13.2 2.1 copy-start.6
  107.2 1.0 copy-start.1
  107.2 1.0 copy-start.4
  107.2 108.5 %reduce-scatter.3.cloned.1.call-start = ((), (), s32[]{:S(2)}) async-start(), calls=%async_computation.2 | async-start | bytes 2621440 | tf_op jit(solution)/shard_map/reduce_scatter | solution.py:507
  108.2 2.2 copy-start.2
  110.4 2.2 copy-start.3
  179.7 3.3 %copy-start.8 = (f32[2]{0:T(128)S(1)}, f32[2]{0:T(128)}, u32[]{:S(2)}) copy-start(f32[2]{0:T(128)} %param.16) | copy-start | bytes 28
  179.7 3.0 %collective-permute-start.1 = (f32[4,128,512]{2,1,0:T(8,128)S(1)}, f32[4,128,512]{2,1,0:T(8,128)S(1)}, u32[]{:S(2)}, u32[]{:S(2)}) collective-permute-start(f32[4,128,512]{2,1,0:T(8,128)S(1)} %slice.65), channel_id=1, source_target_pairs={{0,4},{4,0},{8,12},{12,8},{16,20},{20,16},{24,28},{28,24},{32,36},... | collective-permute-start | bytes 3145736 | tf_op jit(solution)/shard_map/ppermute | solution.py:106
  180.4 2.3 %collective-permute-start = (f32[8,512]{1,0:T(8,128)S(1)}, f32[8,512]{1,0:T(8,128)S(1)}, u32[]{:S(2)}, u32[]{:S(2)}) collective-permute-start(f32[8,512]{1,0:T(8,128)S(1)} %slice.78), channel_id=1, source_target_pairs={{0,4},{4,0},{8,12},{12,8},{16,20},{20,16},{24,28},{28,24},{32,36},... | collective-permute-start | bytes 49160 | tf_op jit(solution)/shard_map/ppermute | solution.py:107
  182.7 0.7 copy-start.9
  185.7 0.7 copy-start.7
Sparse Core Ops, SparseCore 0:
  107.4 53.7 reduce-scatter.4
  185.8 27.7 reduce-scatter.2

commit v4 on v3

v4 whole, which is shorter than its diff:
```python
import functools
import jax
import jax.numpy as jnp
from jax import lax
from jax.experimental import pallas as pl
from jax.experimental.pallas import tpu as pltpu
from jax.sharding import PartitionSpec as P

F32 = jnp.float32
BF = jnp.bfloat16
epsilon = 1e-06
init_lambda = 0.2
LOG2E = 1.4426950408889634
MESH = pl.DeviceIdType.MESH
GROUPS = 8
MAIN = 8
VM = 60 * 1024 * 1024


def whole_kernel(
    main_ref, tail_ref, gate_ref, up_ref, down_ref, key_ref, value_ref, mine_ref, ow_ref, lam_ref, gain_ref,
    mixer_ref, got_ref, last_ref,
    seg_ref, end_ref, g_buf, u_buf, d_buf, part_ref, keys_ref, values_ref, far_ref, near_ref, w_buf,
    ra_ref, rl_ref, rs_ref, rep_ref, tip_ref, acc_ref, max_ref, s_ref, swap_ref,
    mp_ref, ma_ref, ml_ref, ms_ref,
    own_sem, load_sem, put_send, put_recv, near_send, near_recv, far_send, far_recv,
    home_sem, swap_sem, one_send, one_recv, onef_send, onef_recv, two_send, two_recv, twof_send, twof_recv,
    rs_send, rs_recv, mix_send, mix_recv, rep_send, rep_recv, out_sem,
):
    e, x = lax.axis_index("ep"), lax.axis_index("tp")
    n = main_ref.shape[0]
    width = main_ref.shape[2]
    per = n // GROUPS
    right, left = lax.rem(x + 1, 4), lax.rem(x + 3, 4)
    across = lax.rem(x + 2, 4)
    barrier = pltpu.get_barrier_semaphore()
    core, y, z = lax.rem(e, 2), lax.rem(e // 2, 4), e // 8

    def chip(dz, dy):
        return (lax.rem(z + dz, 4) * 4 + lax.rem(y + dy, 4)) * 2 + core, x

    half = key_ref.shape[0] // 2
    home = [
        pltpu.make_async_copy(key_ref, keys_ref.at[z, y], home_sem.at[0]),
        pltpu.make_async_copy(value_ref, values_ref.at[y, z], home_sem.at[1]),
    ]
    swap = pltpu.make_async_remote_copy(
        src_ref=mine_ref, dst_ref=far_ref, send_sem=swap_sem.at[0], recv_sem=swap_sem.at[1],
        device_id=(e ^ 1, x), device_id_type=MESH,
    )
    ends = (keys_ref, values_ref)
    firsts = (key_ref, value_ref)
    inner, outer = (y, z), (z, y)

    def along(w, step, second):
        return chip(step, 0) if (w == 0) == second else chip(0, step)

    def hop(src, dst, sems, w, step, second):
        return pltpu.make_async_remote_copy(
            src_ref=src, dst_ref=dst, send_sem=sems[0], recv_sem=sems[1],
            device_id=along(w, step, second), device_id_type=MESH,
        )

    def rows_of(g):
        return pl.ds(g * half, half)

    def arrival(dst, sem):
        return pltpu.make_async_copy(dst, dst, sem)

    def one_near(w, g, d):
        dst = ends[w].at[outer[w], inner[w], rows_of(g)]
        return hop(firsts[w].at[rows_of(g)], dst, (one_send.at[w, d, g], one_recv.at[w, d, g]), w, 1 if d == 0 else 3, False)

    def one_slot(w, g, step):
        return ends[w].at[outer[w], lax.rem(inner[w] + step, 4), rows_of(g)]

    def one_came(w, g, d):
        return arrival(one_slot(w, g, 3 if d == 0 else 1), one_recv.at[w, d, g])

    def one_far(w, g):
        part = one_slot(w, g, 3 if g == 0 else 1)
        return hop(part, part, (onef_send.at[w, g], onef_recv.at[w, g]), w, 1 if g == 0 else 3, False)

    def two_slot(w, r, step):
        return ends[w].at[lax.rem(outer[w] + step, 4), lax.rem(inner[w] + r, 4)]

    def two_near(w, r, d):
        src = firsts[w] if r == 0 else two_slot(w, r, 0)
        return hop(src, two_slot(w, r, 0), (two_send.at[w, d, r], two_recv.at[w, d, r]), w, 1 if d == 0 else 3, True)

    def two_came(w, r, d):
        return arrival(two_slot(w, r, 3 if d == 0 else 1), two_recv.at[w, d, r])

    def via(r):
        return 0 if r in (0, 1) else 1

    def two_far(w, r):
        d = via(r)
        part = two_slot(w, r, 3 if d == 0 else 1)
        return hop(part, part, (twof_send.at[w, r], twof_recv.at[w, r]), w, 1 if d == 0 else 3, True)

    def spread_first():
        for w in range(2):
            for g in range(2):
                for d in range(2):
                    one_near(w, g, d).start()
        for w in range(2):
            for d in range(2):
                two_near(w, 0, d).start()

    def spread_near():
        for w in range(2):
            for g in range(2):
                one_came(w, g, g).wait()
                one_far(w, g).start()
        for r in (1, 3):
            for w in range(2):
                one_came(w, 1 - (0 if r == 3 else 1), 0 if r == 3 else 1).wait()
                for d in range(2):
                    two_near(w, r, d).start()

    def spread_across():
        for w in range(2):
            for g in range(2):
                arrival(one_slot(w, g, 2), onef_recv.at[w, g]).wait()
            for d in range(2):
                two_near(w, 2, d).start()

    def spread_relay(r):
        for w in range(2):
            two_came(w, r, via(r)).wait()
            two_far(w, r).start()

    def greet(k, _):
        pl.semaphore_signal(barrier, inc=1, device_id=(e ^ k, x), device_id_type=MESH)
        return 0

    lax.fori_loop(1, n, greet, 0)
    for peer in (right, left, across):
        pl.semaphore_signal(barrier, inc=1, device_id=(e, peer), device_id_type=MESH)
    pl.semaphore_wait(barrier, n + 2)

    pairs = ((main_ref, seg_ref), (tail_ref, end_ref))
    own = [pltpu.make_async_copy(src.at[0], dst.at[x, 0], own_sem.at[w]) for w, (src, dst) in enumerate(pairs)]
    for c in own:
        c.start()
    for g in range(GROUPS):
        def put(k, _, g=g):
            for w, (src, dst) in enumerate(pairs):
                pltpu.make_async_remote_copy(
                    src_ref=src.at[k], dst_ref=dst.at[x, k], send_sem=put_send.at[w], recv_sem=put_recv.at[w, g],
                    device_id=(e ^ k, x), device_id_type=MESH,
                ).start()
            return 0

        lax.fori_loop(max(1, g * per), g * per + per, put, 0)
    swap.start()
    loads = [
        pltpu.make_async_copy(src, dst, load_sem.at[k])
        for k, (src, dst) in enumerate(
            ((gate_ref, g_buf), (up_ref, u_buf), (down_ref, d_buf), (mine_ref, near_ref), (ow_ref, w_buf))
        )
    ]
    for c in loads + home:
        c.start()
    for c in own:
        c.wait()

    def span(g):
        return pl.ds(g * per, per)

    def near(w, g, d):
        part = pairs[w][1].at[x, span(g)]
        return pltpu.make_async_remote_copy(
            src_ref=part, dst_ref=part, send_sem=near_send.at[w, d, g], recv_sem=near_recv.at[w, d, g],
            device_id=(e, right if d == 0 else left), device_id_type=MESH,
        )

    def came(w, g, d):
        part = pairs[w][1].at[left if d == 0 else right, span(g)]
        return pltpu.make_async_copy(part, part, near_recv.at[w, d, g])

    def far(w, g):
        d = g % 2
        part = pairs[w][1].at[left if d == 0 else right, span(g)]
        return pltpu.make_async_remote_copy(
            src_ref=part, dst_ref=part, send_sem=far_send.at[w, g], recv_sem=far_recv.at[w, g],
            device_id=(e, right if d == 0 else left), device_id_type=MESH,
        )

    def relay(g):
        for w in range(2):
            came(w, g, g % 2).wait()
            far(w, g).start()

    for g in range(GROUPS):
        first = 1 if g == 0 else g * per
        for w, (src, dst) in enumerate(pairs):
            landed = dst.at[x, pl.ds(first, g * per + per - first)]
            pltpu.make_async_copy(landed, landed, put_recv.at[w, g]).wait()
        for w in range(2):
            for d in range(2):
                near(w, g, d).start()
    spread_first()
    for g in range(GROUPS - 2):
        relay(g)
    for c in loads:
        c.wait()

    def scatter(block, half, a_ref, l_ref, t_ref, sends, recvs):
        def piece(j, hh):
            return block.at[j, pl.ds(hh * half, half)]

        def move(src, dst, k, d):
            return pltpu.make_async_remote_copy(
                src_ref=src, dst_ref=dst, send_sem=sends.at[k, d], recv_sem=recvs.at[k, d],
                device_id=(e, right if d == 0 else left), device_id_type=MESH,
            )

        def away(d):
            return move(piece(across, d), a_ref.at[d], 0, d)

        def plain(d):
            return move(piece(right if d == 0 else left, 1 - d), l_ref.at[d, 1 - d], 1, d)

        def summed(d):
            return move(t_ref.at[d], l_ref.at[d, d], 2, d)

        def join(d):
            away(d).wait_recv()
            j = right if d == 0 else left
            t_ref[d] = (a_ref[d].astype(F32) + block[j, pl.ds(d * half, half), :].astype(F32)).astype(BF)
            summed(d).start()

        def total(hh):
            return (
                block[x, pl.ds(hh * half, half), :].astype(F32) + l_ref[0, hh].astype(F32) + l_ref[1, hh].astype(F32)
            ).astype(BF)

        def landed():
            for d in range(2):
                plain(d).wait_recv()
                summed(d).wait_recv()

        def done():
            for d in range(2):
                away(d).wait_send()
                plain(d).wait_send()
                summed(d).wait_send()

        return away, plain, join, total, landed, done

    rows = n * (MAIN + 2)
    rs_away, rs_plain, rs_join, rs_total, rs_landed, rs_done = scatter(
        part_ref, rows // 2, ra_ref, rl_ref, rs_ref, rs_send, rs_recv
    )

    def expert(t, _):
        @pl.when(t == 1)
        def _():
            for g in range(GROUPS - 2, GROUPS):
                relay(g)
            for w in range(2):
                for g in range(0, GROUPS, 2):
                    came(w, g, 1).wait()

        @pl.when(t == 2)
        def _():
            rs_plain(0).start()
            for w in range(2):
                for g in range(1, GROUPS, 2):
                    came(w, g, 0).wait()
            spread_near()

        @pl.when(t == 3)
        def _():
            rs_plain(1).start()
            spread_across()
            for w in range(2):
                for g in range(GROUPS):
                    part = pairs[w][1].at[across, span(g)]
                    pltpu.make_async_copy(part, part, far_recv.at[w, g]).wait()

        j = lax.rem(x + turn(t), 4)
        tokens = jnp.concatenate(
            [seg_ref[j].reshape(n * MAIN, width), end_ref[j].reshape(n * 2, width)], axis=0
        )
        gate = jnp.dot(tokens, g_buf[...], preferred_element_type=F32)
        up = jnp.dot(tokens, u_buf[...], preferred_element_type=F32)
        hidden = (gate / (1.0 + jnp.exp(-gate)) * up).astype(BF)
        part_ref[j] = jnp.dot(hidden, d_buf[...], preferred_element_type=F32).astype(BF)
        return 0

    lax.fori_loop(0, 4, expert, 0)
    for d in range(2):
        rs_away(d).start()
    spread_relay(0)

    ones = jnp.ones((16, 256), BF)
    row = lax.broadcasted_iota(jnp.int32, (128, 1), 0)
    swap.wait_recv()
    for c in home:
        c.wait()
    acc_ref[...] = jnp.zeros_like(acc_ref)
    max_ref[...] = jnp.full(max_ref.shape, -1e30, F32)

    def queries_of(c):
        h, i = c // 2, c % 2
        both = jnp.concatenate([near_ref[128 * h : 128 * h + 128], far_ref[128 * h : 128 * h + 128]], axis=1)
        return jnp.where((row // 64) == i, both, jnp.zeros_like(both))

    def score(t, c):
        h = c // 2
        k = keys_ref[lax.rem(z + turn(t // 4), 4), lax.rem(y + turn(t % 4), 4), :, 128 * h : 128 * h + 128]
        return jnp.dot(k, queries_of(c), preferred_element_type=F32)

    def finish(t, c, s):
        h = c // 2
        zz, yy = lax.rem(z + turn(t // 4), 4), lax.rem(y + turn(t % 4), 4)
        before = max_ref[c]
        top = jnp.maximum(before, jnp.max(s, axis=0, keepdims=True))
        p = jnp.exp2((s - top[:1]) * LOG2E).astype(BF)
        add = 0.0
        for k in range(2):
            lo = 256 * k + 128 * h
            vt = jnp.concatenate([values_ref[yy, zz, lo : lo + 128, :], ones], axis=0)
            add = add + jnp.dot(vt, p[256 * k : 256 * k + 256], preferred_element_type=F32)
        acc_ref[c] = acc_ref[c] * jnp.exp2((before - top) * LOG2E)[:1] + add
        max_ref[c] = top

    def rest(w, r):
        two_came(w, r, 1 - via(r)).wait()

    def reach(w, r):
        arrival(two_slot(w, r, 2), twof_recv.at[w, r]).wait()

    pieces = ((rep_ref, got_ref), (tip_ref, last_ref))

    def answer():
        rs_landed()
        low, high = rs_total(0), rs_total(1)
        rep_ref[...] = jnp.concatenate([low, high[: n * MAIN - rows // 2]], axis=0).reshape(n, MAIN, width)
        tip_ref[...] = high[n * MAIN - rows // 2 :].reshape(n, 2, width)
        got_ref[0] = rep_ref[0]
        last_ref[0] = tip_ref[0]

        def put(k, _):
            for w, (src, dst) in enumerate(pieces):
                pltpu.make_async_remote_copy(
                    src_ref=src.at[k], dst_ref=dst.at[k], send_sem=rep_send.at[w], recv_sem=rep_recv.at[w],
                    device_id=(e ^ k, x), device_id_type=MESH,
                ).start()
            return 0

        lax.fori_loop(1, n, put, 0)

    events = {
        0: lambda: rest(1, 0),
        1: lambda: spread_relay(1),
        2: lambda: reach(1, 0),
        3: lambda: (rest(0, 0), spread_relay(3)),
        4: lambda: (rest(0, 1), rest(1, 1)),
        5: lambda: (spread_relay(2), rs_join(0), rs_join(1)),
        6: lambda: reach(1, 1),
        9: lambda: (rest(0, 3), rest(1, 3)),
        10: lambda: (rest(0, 2), reach(1, 3)),
        11: lambda: reach(0, 0),
        12: lambda: (reach(0, 1), answer()),
        13: lambda: (reach(0, 3), rest(1, 2)),
        14: lambda: (reach(0, 2), reach(1, 2)),
    }
    s_ref[0] = score(0, 0)

    def attend_block(t, _):
        for k, act in events.items():
            @pl.when(t == k)
            def _(act=act):
                act()
        for c in range(4):
            s_ref[(c + 1) % 2] = score(t, c + 1) if c < 3 else score(jnp.minimum(t + 1, 15), 0)
            finish(t, c, s_ref[c % 2])
        return 0

    lax.fori_loop(0, 16, attend_block, 0)

    mid = acc_ref.shape[2] // 2
    acc_ref[:, 136:144, :] = max_ref[...]
    trade = pltpu.make_async_remote_copy(
        src_ref=acc_ref.at[:, :, pl.ds(mid, mid)], dst_ref=swap_ref, send_sem=out_sem.at[0], recv_sem=out_sem.at[1],
        device_id=(e ^ 1, x), device_id_type=MESH,
    )
    trade.start()
    trade.wait_recv()
    heads = []
    for h in range(2):
        maps = []
        for i in range(2):
            c = 2 * h + i
            a_max, b_max = acc_ref[c, 136:137, :mid], swap_ref[c, 136:137, :]
            top = jnp.maximum(a_max, b_max)
            fa, fb = jnp.exp2((a_max - top) * LOG2E), jnp.exp2((b_max - top) * LOG2E)
            totals = acc_ref[c, 128:129, :mid] * fa + swap_ref[c, 128:129, :] * fb
            maps.append((acc_ref[c, :128, :mid] * fa + swap_ref[c, :128, :] * fb) / totals)
        head = maps[0] - lam_ref[h : h + 1, :] * maps[1]
        mean = jnp.mean(head * head, axis=0, keepdims=True)
        heads.append((head * lax.rsqrt(mean + epsilon) * gain_ref[...] * (1.0 - init_lambda)).astype(BF))
    attended = jnp.concatenate(heads, axis=0).astype(F32).T.astype(BF)
    tokens = mp_ref.shape[1]
    for j in range(4):
        mp_ref[j] = jnp.dot(
            attended[j * tokens : j * tokens + tokens], w_buf[...], preferred_element_type=F32
        ).astype(BF)
    mx_away, mx_plain, mx_join, mx_total, mx_landed, mx_done = scatter(
        mp_ref, tokens // 2, ma_ref, ml_ref, ms_ref, mix_send, mix_recv
    )
    for d in range(2):
        mx_away(d).start()
    for d in range(2):
        mx_plain(d).start()
    for d in range(2):
        mx_join(d)
    for w, (src, dst) in enumerate(pieces):
        moved = dst.at[pl.ds(1, n - 1)]
        pltpu.make_async_copy(moved, moved, rep_recv.at[w]).wait()
        pltpu.make_async_copy(moved, moved, rep_send.at[w]).wait()
    mx_landed()
    mixer_ref[...] = jnp.concatenate([mx_total(0), mx_total(1)], axis=0)

    mx_done()
    rs_done()
    trade.wait_send()
    swap.wait_send()
    for w, (src, dst) in enumerate(pairs):
        sent = dst.at[x, pl.ds(1, n - 1)]
        pltpu.make_async_copy(sent, sent, put_send.at[w]).wait()
        for g in range(GROUPS):
            for d in range(2):
                near(w, g, d).wait_send()
            far(w, g).wait_send()
        for r in range(4):
            two_far(w, r).wait_send()
            for d in range(2):
                two_near(w, r, d).wait_send()
        for g in range(2):
            one_far(w, g).wait_send()
            for d in range(2):
                one_near(w, g, d).wait_send()


def turn(t):
    return t + (t // 2) * (1 - 2 * (t % 2))


def whole(main, tail, gate, up, down, key, value, mine, out_weight, lam, gain):
    n, _, width = main.shape
    dma = pltpu.SemaphoreType.DMA
    hbm, vmem = pl.BlockSpec(memory_space=pl.ANY), pl.BlockSpec(memory_space=pltpu.VMEM)
    rows = n * (MAIN + 2)
    local = mine.shape[1]

    def bf(*shape):
        return pltpu.VMEM(shape, BF)

    def fl(*shape):
        return pltpu.VMEM(shape, F32)

    return pl.pallas_call(
        whole_kernel,
        out_shape=(
            jax.ShapeDtypeStruct((local // 4, width), BF),
            jax.ShapeDtypeStruct(main.shape, BF),
            jax.ShapeDtypeStruct(tail.shape, BF),
        ),
        in_specs=[hbm] * 9 + [vmem] * 2,
        out_specs=(vmem,) * 3,
        scratch_shapes=[
            bf(4, n, MAIN, width), bf(4, n, 2, width), bf(*gate.shape), bf(*up.shape), bf(*down.shape),
            bf(4, rows, width), bf(4, 4, *key.shape), bf(4, 4, *value.shape), bf(*mine.shape), bf(*mine.shape),
            bf(*out_weight.shape),
            bf(2, rows // 2, width), bf(2, 2, rows // 2, width), bf(2, rows // 2, width),
            bf(n, MAIN, width), bf(n, 2, width),
            fl(4, 144, 2 * local), fl(4, 8, 2 * local), fl(2, 512, 2 * local), fl(4, 144, local),
            bf(4, local // 4, width), bf(2, local // 8, width), bf(2, 2, local // 8, width), bf(2, local // 8, width),
            dma((2,)), dma((5,)), dma((2,)), dma((2, GROUPS)), dma((2, 2, GROUPS)), dma((2, 2, GROUPS)),
            dma((2, GROUPS)), dma((2, GROUPS)),
            dma((2,)), dma((2,)), dma((2, 2, 2)), dma((2, 2, 2)), dma((2, 2)), dma((2, 2)),
            dma((2, 2, 4)), dma((2, 2, 4)), dma((2, 4)), dma((2, 4)),
            dma((3, 2)), dma((3, 2)), dma((3, 2)), dma((3, 2)), dma((2,)), dma((2,)), dma((2,)),
        ],
        compiler_params=pltpu.CompilerParams(
            collective_id=0, has_side_effects=True, vmem_limit_bytes=VM
        ),
        name="layer",
    )(main, tail, gate, up, down, key, value, mine, out_weight, lam, gain)


def per_device(
    queries, key_rows, value_rows, lambdas, head_gain, out_weight, moe_input, moe_gain,
    routes, route_logits, expert_gate, expert_up, expert_down,
):
    width = out_weight.shape[1]
    token_count, top_count = routes.shape
    n = lax.axis_size("ep")
    moe_float = moe_input.astype(F32)
    normed = (
        moe_float
        * lax.rsqrt(jnp.mean(moe_float * moe_float, axis=-1, keepdims=True) + epsilon)
        * moe_gain
    ).astype(BF)
    gate_weights = jax.nn.softmax(route_logits, axis=-1)
    flat_routes = routes.reshape(-1)
    chosen = (flat_routes[:, None] == jnp.arange(n, dtype=jnp.int32)[None, :]).astype(jnp.int32)
    rank = jnp.sum((jnp.cumsum(chosen, axis=0) - chosen) * chosen, axis=1)
    step = flat_routes ^ lax.axis_index("ep")
    place = jnp.where(rank < MAIN, step * MAIN + rank, n * MAIN + step * 2 + rank - MAIN)
    place = place.reshape(token_count, top_count)
    slots = jnp.arange(n * (MAIN + 2), dtype=jnp.int32)
    dispatch = jnp.any(place[None, :, :] == slots[:, None, None], axis=-1).astype(BF)
    outgoing = jnp.dot(dispatch, normed, preferred_element_type=F32).astype(BF)
    mine = (queries * jnp.asarray(0.125, BF)).T
    values_t = value_rows.T
    value = jnp.concatenate([values_t[:, :256], values_t[:, 256:]], axis=0)
    lam = jnp.broadcast_to(lambdas[:, None], (2, queries.shape[0]))
    mixer_out, got, got_end = whole(
        outgoing[: n * MAIN].reshape(n, MAIN, width), outgoing[n * MAIN :].reshape(n, 2, width),
        expert_gate[0], expert_up[0], expert_down[0], key_rows, value, mine, out_weight, lam, head_gain[:, None],
    )
    weights = jnp.sum(
        jnp.where(place[:, :, None] == slots, gate_weights[:, :, None], 0.0), axis=1
    )
    high = weights.astype(BF)
    low = (weights - high.astype(F32)).astype(BF)
    both = jnp.concatenate([got.reshape(n * MAIN, width), got_end.reshape(n * 2, width)], axis=0)
    expert_out = (
        jnp.dot(high, both, preferred_element_type=F32) + jnp.dot(low, both, preferred_element_type=F32)
    ).astype(BF)
    return (mixer_out, expert_out)


def solution(mesh):
    placed = (
        P("ep", "tp"),
        P("ep", "tp"),
        P("ep", "tp"),
        P("tp"),
        P(),
        P("tp", None),
        P(("ep", "tp"), None),
        P(),
        P(("ep", "tp"), None),
        P(("ep", "tp"), None),
        P("ep", None, "tp"),
        P("ep", None, "tp"),
        P("ep", "tp", None),
    )
    return jax.shard_map(
        per_device,
        mesh=mesh,
        in_specs=placed,
        out_specs=(P(("ep", "tp"), None), P(("ep", "tp"), None)),
        check_vma=False,
    )
```

time: 223 us -> 159 us (0.71)
  Pallas kernels: 182 us -> 142 us
  between operations: 14.3 us -> 0.77 us
  local copies, waits for them, and re-layouts: 12.6 us -> 7.05 us
    pallas_call x3 -> x1, Pallas kernels: 182 us -> 142 us  [whole(): pl.pallas_call(whole_kernel, out_shape=(jax.ShapeDtypeStruct((local // 4,...]
    unnamed x24 -> x20, local copies, waits for them, and re-layouts: 7.33 us -> 1.95 us
  transfers between devices with their start and end apart: 4 -> 0, of which waited for: 1 -> 0; matrix products, arithmetic and copies ran while one was open for 3% -> 0% of each run, Pallas kernels for 41% -> 0%
where the time goes in v4:
time: 159 us
  Pallas kernels  142 us (89%)
  local copies, waits for them, and re-layouts  7.05 us (4%)
  matrix products  4.33 us (3%)
  other arithmetic  4.26 us (3%)
    pallas_call x1, Pallas kernels, whole(): pl.pallas_call(whole_kernel, out_shape=(jax.ShapeDtypeStruct((local // 4,...  142 us

profile of v4, /device:TPU:1, one launch (start us, length us, event | category | flops | bytes accessed | tf_op | source)
XLA Modules:
  0.0 158.5 jit_solution(9362976863702027419)
XLA Ops:
  0.6 0.0 copy-start.1
  0.6 0.8 copy.38
  1.5 0.1 eq.55
  1.6 0.6 reduce-window.6
  2.2 0.2 slice_reduce_fusion
  2.5 0.1 eq.51
  2.6 0.1 fusion.13
  2.7 0.1 reduce_sum.39
  2.9 0.1 copy.41
  2.9 0.7 compare_select_fusion
  3.7 1.2 fusion.1
  4.9 0.0 copy-done.1
  4.9 1.3 convolution_convert_fusion
  6.2 0.0 copy-start.3
  6.2 1.1 slice_bitcast_fusion.main_ref
  7.3 0.0 copy-start.4
  7.3 0.9 reshape.79.tail_ref
  8.2 0.0 copy-done.3
  8.2 0.0 copy-start.6
  8.2 0.0 copy-start.7
  8.2 0.1 copy.44
  8.4 0.7 pad_maximum_fusion.3.value_ref
  9.1 0.0 copy-done.4
  9.1 0.1 copy.45
  9.2 0.7 multiply_bitcast_fusion.mine_ref
  10.0 0.0 copy-done.6
  10.0 0.7 copy.46.gain_ref
  10.7 0.0 copy-done.7
  10.7 0.7 broadcast_in_dim.12.lam_ref
  11.3 0.0 copy-start.5
  11.4 142.1 %layer.1 = (bf16[128,2048]{1,0:T(8,128)(2,1)}, bf16[32,8,2048]{2,1,0:T(8,128)(2,1)}, bf16[32,2,2048]{2,1,0:T(2,128)(2,1)}) custom-call(bf16[32,8,2048]{2,1,0:T(8,128)(2,1)} %slice_bitcast_fusion.main_ref, bf16[32,2,2048]{2,1,0:T(2,128)(2,1)} %reshape.79.tail_ref, bf16[2048,896]{1,0:T(8,128)(2,1)} %bitcast.32, bf16[2048,896]{1,0:T(8,128)(2,1)} %bitcast.33, ...), custom_call_target="tpu_custom_call" | custom-call | tf_op jit(solution)/shard_map/layer/pallas_call | solution.py:467
  153.5 1.0 reshape.81
  154.5 0.0 copy-done.5
  154.6 0.0 copy-start
  154.6 1.8 %fusion.4 = f32[128,2048]{1,0:T(8,128)S(1)} fusion(bf16[64,2048]{1,0:T(8,128)(2,1)S(1)} %reshape.81, bf16[256,2048]{1,0:T(8,128)(2,1)} %bitcast.30, f32[128,320]{0,1:T(8,128)S(1)} %select_reduce_fusion), kind=kOutput, calls=%fused_computation.10 | convolution fusion | flops 170434560 | bytes 2523136 | tf_op jit(solution)/shard_map/dot_general | solution.py:535
  156.4 0.0 copy-done
  156.4 0.0 copy-start.2
  156.4 1.3 fusion
  157.7 0.0 copy-done.2
  157.7 0.8 copy.50
  (11 shorter events, 0.2 us)
Async XLA Ops:
  0.6 4.3 %copy-start.1 = (bf16[128,2048]{1,0:T(8,128)(2,1)S(1)}, bf16[128,2048]{1,0:T(8,128)(2,1)}, u32[]{:S(2)}) copy-start(bf16[128,2048]{1,0:T(8,128)(2,1)} %param.19) | copy-start | bytes 1572868
  6.2 2.0 %copy-start.3 = (bf16[512,256]{1,0:T(8,128)(2,1)S(1)}, bf16[512,256]{1,0:T(8,128)(2,1)}, u32[]{:S(2)}) copy-start(bf16[512,256]{1,0:T(8,128)(2,1)} %param.15) | copy-start | bytes 786436
  7.3 1.8 %copy-start.4 = (bf16[512,256]{1,0:T(8,128)(2,1)S(1)}, bf16[512,256]{1,0:T(8,128)(2,1)}, u32[]{:S(2)}) copy-start(bf16[512,256]{1,0:T(8,128)(2,1)} %param.13) | copy-start | bytes 786436
  8.2 1.8 %copy-start.6 = (f32[128]{0:T(128)S(1)}, f32[128]{0:T(128)}, u32[]{:S(2)}) copy-start(f32[128]{0:T(128)} %param.17) | copy-start | bytes 1540
  8.2 2.5 %copy-start.7 = (f32[2]{0:T(128)S(1)}, f32[2]{0:T(128)}, u32[]{:S(2)}) copy-start(f32[2]{0:T(128)} %param.16) | copy-start | bytes 28
  11.3 143.2 %copy-start.5 = (f32[128,2]{0,1:T(2,128)S(1)}, f32[128,2]{0,1:T(2,128)}, u32[]{:S(2)}) copy-start(f32[128,2]{0,1:T(2,128)} %param.22) | copy-start | bytes 3076
  154.6 1.8 %copy-start = (bf16[32,8,2048]{2,1,0:T(8,128)(2,1)S(1)}, bf16[32,8,2048]{2,1,0:T(8,128)(2,1)}, u32[]{:S(2)}) copy-start(bf16[32,8,2048]{2,1,0:T(8,128)(2,1)} %get-tuple-element.6) | copy-start | bytes 3145732
  156.4 1.3 copy-start.2
